TPU v7x, 1024 devices: a whole 4x4x32 slice. The times are simulated.
1024 devices in a mesh: sp: 128 (over z, y), tp: 8 (over x, core).
Axes of the slice: x: 4, y: 4, z: 32, core: 2. Of those that a mesh axis runs over, the one named last changes fastest.
Arguments:
- tokens: bfloat16 [4, 8192, 2048], P(None, ('sp', 'tp')), may hold values from -6 to 6
- in_gain: float32 [2048], replicated, may hold values from 0.1 to 1.9
- gate_weight: bfloat16 [2048, 1024], P(None, 'tp'), may hold values from -0.125 to 0.125
- input_weight: bfloat16 [2048, 1024], P(None, 'tp'), may hold values from -0.125 to 0.125
- key_weight: bfloat16 [2048, 512], P(None, 'tp'), may hold values from -0.125 to 0.125
- query_weight: bfloat16 [2048, 512], P(None, 'tp'), may hold values from -0.125 to 0.125
- step_weight: bfloat16 [2048, 16], replicated, may hold values from -0.125 to 0.125
- conv_input: float32 [4, 1024], P(None, 'tp'), may hold values from -3 to 3
- conv_key: float32 [4, 512], P(None, 'tp'), may hold values from -3 to 3
- conv_query: float32 [4, 512], P(None, 'tp'), may hold values from -3 to 3
- step_bias: float32 [16], P('tp'), may hold values from -5 to 1
- decay_rate: float32 [16], P('tp'), may hold values from 0 to 1, as said below
- decay_extra: float32 [4, 16, 8192], P(None, 'tp', 'sp'), may hold values from -0.7 to 0, as said below
- out_gain: float32 [1024], P('tp'), may hold values from 0.1 to 1.9
- out_weight: bfloat16 [1024, 2048], replicated, may hold values from -0.1875 to 0.1875
Outputs:
- output: bfloat16 [4, 8192, 2048], P(None, ('sp', 'tp'))
Inputs may be any that keep to these rules, and one draw needn't show every extreme that they name: `decay_rate`: one positive rate a head. `decay_extra`: never positive.
All inputs are finite; a program needn't handle non-finite values.
Results may differ from a plain program's by a relative error of at most 0.0072.
Values may be sent and summed in bfloat16 or wider, within the bound.
A program may use at most 128 MiB of HBM per device.

v0:
```python
import jax
import jax.numpy as jnp
from jax import lax
from jax.sharding import PartitionSpec as P

HEAD_TOTAL = 16
HEAD_DIM = 64
GROUPS = 8
STATE = 64
CONV = 4
BLOCK = 64


NORM_EPS = 1e-06
PRECISE = lax.Precision.HIGHEST


def in_order(tiles, dim):
    tiles = jnp.moveaxis(tiles, 0, dim)
    lengths = tiles.shape
    return tiles.reshape(*lengths[:dim], lengths[dim] * lengths[dim + 1], *lengths[dim + 2 :])


def from_everyone(array, axis):
    length = lax.axis_size(axis)
    return lax.all_to_all(
        jnp.broadcast_to(array[None], (length, *array.shape)), axis, 0, 0, tiled=True
    )


def collect(array, axis, dim):
    return in_order(from_everyone(array, axis), dim)


def from_behind(array, axis, by):
    length = lax.axis_size(axis)
    pairs = [(i, i + by) for i in range(length) if 0 <= i + by < length]
    return lax.ppermute(array, axis, pairs)


def carried_in(array, axis, combine, identity):
    length, place = (lax.axis_size(axis), lax.axis_index(axis))
    everything = jax.tree.map(lambda part: lax.all_gather(part, axis), array)
    start = jax.tree.map(
        lambda part, zero: jnp.broadcast_to(jnp.asarray(zero, part.dtype), part.shape),
        array,
        identity,
    )

    def step(k, before):
        reached = k < place
        new = combine(before, jax.tree.map(lambda part: part[k], everything))
        return jax.tree.map(lambda a, b: jnp.where(reached, a, b), new, before)

    return lax.fori_loop(0, length, step, start)


def rms_rows(values, gain_row):
    mean_sq = jnp.mean(values * values, axis=-1, keepdims=True)
    return values * lax.rsqrt(mean_sq + NORM_EPS) * gain_row


def causal_blend(rim_rows, local_rows, weights):
    length = local_rows.shape[1]
    padded = jnp.concatenate([rim_rows, local_rows], axis=1).astype(jnp.float32)
    summed_rows = padded[:, 0:length, :] * weights[0]
    for offset in range(1, weights.shape[0]):
        summed_rows = summed_rows + padded[:, offset : offset + length, :] * weights[offset]
    return jax.nn.silu(summed_rows)


def local_pass(scaled_x, keys_b, readout_vectors, log_decay):
    seq_count, seg_len, heads_here = (scaled_x.shape[0], scaled_x.shape[1], scaled_x.shape[2])
    blocks_here = seg_len // BLOCK
    ratio_heads = HEAD_TOTAL // GROUPS

    def to_blocks(tensor):
        return tensor.reshape((seq_count, blocks_here, BLOCK) + tensor.shape[2:])

    x_blocks = to_blocks(scaled_x)
    b_blocks = to_blocks(keys_b)
    c_blocks = to_blocks(readout_vectors)
    inside_block = jnp.cumsum(to_blocks(log_decay), axis=2)
    causal = jnp.tril(jnp.ones((BLOCK, BLOCK), bool))[None, None, :, :, None]
    spread_log = inside_block[:, :, :, None, :] - inside_block[:, :, None, :, :]
    decay_matrix = jnp.where(causal, jnp.exp(jnp.where(causal, spread_log, 0.0)), 0.0)
    scores = jnp.einsum("sblgn,sbtgn->sbltg", c_blocks, b_blocks, precision=PRECISE)
    scores = jnp.repeat(scores, ratio_heads, axis=4)
    key_heads = jnp.repeat(b_blocks, ratio_heads, axis=3)
    query_heads = jnp.repeat(c_blocks, ratio_heads, axis=3)
    inner_part = jnp.einsum(
        "sblth,sbthp->sblhp", scores * decay_matrix, x_blocks, precision=PRECISE
    )
    tail_weight = jnp.exp(inside_block[:, :, -1:, :] - inside_block)
    block_states = jnp.einsum(
        "sblhn,sblhp->sbhpn", key_heads, x_blocks * tail_weight[..., None], precision=PRECISE
    )
    block_totals = inside_block[:, :, -1, :]
    running = jnp.zeros((seq_count, heads_here, HEAD_DIM, STATE), jnp.float32)
    entering = [running]
    running = jnp.exp(block_totals[:, 0])[:, :, None, None] * running + block_states[:, 0]
    entering_states = jnp.stack(entering, axis=1)
    forwarded_portion = jnp.einsum(
        "sblhn,sbhpn->sblhp", query_heads, entering_states, precision=PRECISE
    )
    forwarded_portion = forwarded_portion * jnp.exp(inside_block)[..., None]
    local_out = (inner_part + forwarded_portion).reshape(seq_count, seg_len, heads_here, HEAD_DIM)
    decay_total = jnp.exp(jnp.sum(block_totals, axis=1))
    prefix_log = jnp.cumsum(log_decay, axis=1)
    return (local_out, decay_total, running, prefix_log)


def read_in(local_out, readout_vectors, prefix_log, incoming):
    query_heads = jnp.repeat(readout_vectors, HEAD_TOTAL // GROUPS, axis=2)
    carried = jnp.einsum("slhn,shpn->slhp", query_heads, incoming, precision=PRECISE)
    return local_out + carried * jnp.exp(prefix_log)[..., None]


def combine(preceding_portion, latter):
    return (
        preceding_portion[0] * latter[0],
        latter[0][:, :, None, None] * preceding_portion[1] + latter[1],
    )


def body(
    tokens,
    in_gain,
    gate_weight,
    input_weight,
    key_weight,
    query_weight,
    step_weight,
    conv_input,
    conv_key,
    conv_query,
    step_bias,
    decay_rate,
    decay_extra,
    out_gain,
    out_weight,
):
    normed = rms_rows(tokens.astype(jnp.float32), in_gain).astype(jnp.bfloat16)
    joined_weight = jnp.concatenate(
        [gate_weight, input_weight, key_weight, query_weight, step_weight], axis=1
    )
    token_segment = collect(normed, "tp", 1)
    seq_count = token_segment.shape[0]
    row_count = token_segment.shape[1]
    result = jnp.dot(
        token_segment.reshape(seq_count * row_count, token_segment.shape[2]),
        joined_weight,
        preferred_element_type=jnp.float32,
    )
    projected = result.astype(jnp.bfloat16).reshape(seq_count, row_count, joined_weight.shape[1])
    seq_count, seg_len = (projected.shape[0], projected.shape[1])
    inner_here = gate_weight.shape[1]
    state_cols = key_weight.shape[1]
    heads_here = step_bias.shape[0]
    gate_in = projected[:, :, :inner_here]
    conv_in = projected[:, :, inner_here : 2 * inner_here + 2 * state_cols]
    step_all = projected[:, :, 2 * inner_here + 2 * state_cols :]
    rim_rows = from_behind(conv_in[:, seg_len - CONV + 1 :, :], "sp", 1)
    conv_weights = jnp.concatenate([conv_input, conv_key, conv_query], axis=1)
    conv_out = causal_blend(rim_rows, conv_in, conv_weights)
    conv_values = conv_out[:, :, :inner_here].reshape(seq_count, seg_len, heads_here, HEAD_DIM)
    keys_b = conv_out[:, :, inner_here : inner_here + state_cols].reshape(
        seq_count, seg_len, state_cols // STATE, STATE
    )
    readout_vectors = conv_out[:, :, inner_here + state_cols :].reshape(
        seq_count, seg_len, state_cols // STATE, STATE
    )
    own_steps = lax.dynamic_slice_in_dim(step_all, lax.axis_index("tp") * heads_here, heads_here, 2)
    step_size = jax.nn.softplus(own_steps.astype(jnp.float32) + step_bias)
    log_decay = -step_size * decay_rate + jnp.transpose(decay_extra, (0, 2, 1))
    scaled_x = conv_values * step_size[..., None]
    local_out, decay_total, final_state, prefix_log = local_pass(
        scaled_x, keys_b, readout_vectors, log_decay
    )
    incoming = carried_in(
        (decay_total, final_state),
        "sp",
        combine,
        (jnp.ones_like(decay_total), jnp.zeros_like(final_state)),
    )
    blended_heads = read_in(local_out, readout_vectors, prefix_log, incoming[1])
    gated_rows = blended_heads.reshape(seq_count, seg_len, inner_here) * jax.nn.silu(
        gate_in.astype(jnp.float32)
    )
    group_width = HEAD_TOTAL // GROUPS * HEAD_DIM
    groups_here = inner_here // group_width
    normed_out = rms_rows(
        gated_rows.reshape(seq_count, seg_len, groups_here, group_width),
        out_gain.reshape(groups_here, group_width),
    )
    normed_out = normed_out.reshape(seq_count, seg_len, inner_here).astype(jnp.bfloat16)
    token_rows = lax.all_to_all(normed_out, "tp", split_axis=1, concat_axis=2, tiled=True)
    result = jnp.dot(
        token_rows.reshape(token_rows.shape[0] * token_rows.shape[1], token_rows.shape[2]),
        out_weight,
        preferred_element_type=jnp.float32,
    )
    return result.astype(jnp.bfloat16).reshape(
        token_rows.shape[0], token_rows.shape[1], out_weight.shape[1]
    )


def solution(mesh):
    placed = (
        P(None, ("sp", "tp"), None),
        P(),
        P(None, "tp"),
        P(None, "tp"),
        P(None, "tp"),
        P(None, "tp"),
        P(),
        P(None, "tp"),
        P(None, "tp"),
        P(None, "tp"),
        P("tp"),
        P("tp"),
        P(None, "tp", "sp"),
        P("tp"),
        P(),
    )
    return jax.shard_map(
        body, mesh=mesh, in_specs=placed, out_specs=P(None, ("sp", "tp"), None), check_vma=False
    )
```

profile of v0, /device:TPU:1, one launch (start us, length us, event | category | flops | bytes accessed | tf_op | source)
XLA Modules:
  0.0 602.5 jit_solution(16381188262270441161)
XLA Ops:
  6.5 1.1 fusion.7
  8.6 1.1 broadcast_in_dim.18
  9.7 17.7 %all-to-all-start = ((bf16[8,4,8,2048]{3,2,1,0:T(8,128)(2,1)}), bf16[8,4,8,2048]{3,2,1,0:T(8,128)(2,1)S(1)}, u32[]{:S(2)}, u32[]{:S(2)}) async-start(bf16[8,4,8,2048]{3,2,1,0:T(8,128)(2,1)} %broadcast_in_dim.18), calls=%async_computation | async-start | bytes 2097152 | tf_op jit(solution)/shard_map/all_to_all | solution.py:26
  27.4 2.0 copy.82
  31.4 4.0 concatenate.9
  35.6 6.8 %all-to-all-done = bf16[8,4,8,2048]{3,2,1,0:T(8,128)(2,1)S(1)} async-done(((bf16[8,4,8,2048]{3,2,1,0:T(8,128)(2,1)}), bf16[8,4,8,2048]{3,2,1,0:T(8,128)(2,1)S(1)}, u32[]{:S(2)}, u32[]{:S(2)}) %all-to-all-start) | async-done | bytes 1048608 | tf_op jit(solution)/shard_map/all_to_all | solution.py:26
  44.4 1.3 collective-permute-start
  47.0 1.1 convolution_add_fusion
  48.4 161.0 %all-gather = f32[512,1,1,2]{3,2,1,0:T(1,128)S(1)} all-gather(f32[4,1,1,2]{3,2,1,0:T(1,128)S(1)} %get-tuple-element.153), channel_id=2, replica_groups=mesh['sp'=128,'tp'=8] {'sp'}, dimensions={0}, use_global_device_ids=true | all-gather | bytes 4128 | tf_op jit(solution)/shard_map/all_gather | solution.py:43
  212.4 217.9 %all-gather.4.cloned.1.call-done = f32[512,2,64,64]{3,2,1,0:T(8,128)} async-done(((f32[4,2,64,64]{3,2,1,0:T(8,128)}), f32[512,2,64,64]{3,2,1,0:T(8,128)}) %all-gather.4.cloned.1.call-update) | async-done | bytes 16777232 | tf_op jit(solution)/shard_map/all_gather | solution.py:43
  430.2 150.5 %while.14 = (s32[]{:T(128)}, f32[4,2,64,64]{3,2,1,0:T(8,128)S(1)}, s32[]{:T(128)}, f32[128,4,2]{1,2,0:T(2,128)S(1)}, f32[128,4,2,64,64]{4,3,2,1,0:T(8,128)}, /*index=5*/s32[]{:T(128)}, s32[]{:T(128)}) while((s32[]{:T(128)}, f32[4,2,64,64]{3,2,1,0:T(8,128)S(1)}, s32[]{:T(128)}, f32[128,4,2]{1,2,0:T(2,128)S(1)}, ...), condition=%wide.region_3.4_spmd.clone, body=%wide.region_2.3_spmd.clone.sunk | while | flops 131076 | bytes 393489 | solution.py:55
  432.7 1.0 fusion.51
  435.0 1.0 fusion.51
  437.4 1.0 fusion.51
  439.8 1.0 fusion.51
  448.0 1.0 fusion.51
  450.3 1.0 fusion.51
  452.7 1.0 fusion.51
  455.0 1.0 fusion.51
  457.4 1.0 fusion.51
  459.7 1.0 fusion.51
  462.1 1.0 fusion.51
  470.3 1.0 fusion.51
  472.7 1.0 fusion.51
  475.0 1.0 fusion.51
  477.4 1.0 fusion.51
  479.7 1.0 fusion.51
  482.1 1.0 fusion.51
  484.4 1.0 fusion.51
  492.7 1.0 fusion.51
  495.0 1.0 fusion.51
  497.4 1.0 fusion.51
  499.7 1.0 fusion.51
  502.1 1.0 fusion.51
  504.4 1.0 fusion.51
  506.8 1.0 fusion.51
  515.0 1.0 fusion.51
  517.4 1.0 fusion.51
  519.7 1.0 fusion.51
  522.1 1.0 fusion.51
  524.4 1.0 fusion.51
  526.8 1.0 fusion.51
  529.1 1.0 fusion.51
  537.3 1.0 fusion.51
  539.7 1.0 fusion.51
  542.0 1.0 fusion.51
  581.7 10.3 %all_to_all.20 = bf16[4,64,128]{2,0,1:T(4,128)(2,1)S(1)} all-to-all(bf16[4,64,128]{2,0,1:T(4,128)(2,1)S(1)} %copy.103), channel_id=1, replica_groups=mesh['sp'=128,'tp'=8] {'tp'}, dimensions={1} | all-to-all | bytes 131072 | tf_op jit(solution)/shard_map/all_to_all | solution.py:197
  592.0 3.7 fusion.1
  (419 shorter events, 120.8 us)
Async XLA Ops:
  6.5 22.9 %copy-start = (bf16[2048,64]{0,1:T(8,128)(2,1)S(1)}, bf16[2048,64]{0,1:T(8,128)(2,1)}, u32[]{:S(2)}) copy-start(bf16[2048,64]{0,1:T(8,128)(2,1)} %param.22) | copy-start | bytes 786436
  6.5 23.9 %copy-start.1 = (bf16[2048,16]{0,1:T(8,128)(2,1)S(1)}, bf16[2048,16]{0,1:T(8,128)(2,1)}, u32[]{:S(2)}) copy-start(bf16[2048,16]{0,1:T(8,128)(2,1)} %param.23) | copy-start | bytes 196612
  9.7 25.7 %copy-start.3 = (f32[4,64]{1,0:T(4,128)S(1)}, f32[4,64]{1,0:T(4,128)}, u32[]{:S(2)}) copy-start(f32[4,64]{1,0:T(4,128)} %param.26) | copy-start | bytes 3076
  9.7 25.7 %copy-start.4 = (f32[4,64]{1,0:T(4,128)S(1)}, f32[4,64]{1,0:T(4,128)}, u32[]{:S(2)}) copy-start(f32[4,64]{1,0:T(4,128)} %param.25) | copy-start | bytes 3076
  9.7 25.8 %copy-start.5 = (f32[4,128]{1,0:T(4,128)S(1)}, f32[4,128]{1,0:T(4,128)}, u32[]{:S(2)}) copy-start(f32[4,128]{1,0:T(4,128)} %param.24) | copy-start | bytes 6148
  9.7 32.7 %all-to-all-start = ((bf16[8,4,8,2048]{3,2,1,0:T(8,128)(2,1)}), bf16[8,4,8,2048]{3,2,1,0:T(8,128)(2,1)S(1)}, u32[]{:S(2)}, u32[]{:S(2)}) async-start(bf16[8,4,8,2048]{3,2,1,0:T(8,128)(2,1)} %broadcast_in_dim.18), calls=%async_computation | async-start | bytes 2097152 | tf_op jit(solution)/shard_map/all_to_all | solution.py:26
  27.4 402.8 %all-gather.4.cloned.1.call-start = ((), (), s32[]{:S(2)}) async-start(), calls=%async_computation.2 | async-start | bytes 33816576 | tf_op jit(solution)/shard_map/all_gather | solution.py:43
  35.5 8.3 %copy-start.2 = (f32[4,2,64]{2,1,0:T(2,128)S(1)}, f32[4,2,64]{2,1,0:T(2,128)}, u32[]{:S(2)}) copy-start(f32[4,2,64]{2,1,0:T(2,128)} %param.29) | copy-start | bytes 6148
  35.5 8.3 %copy-start.7 = (f32[2]{0:T(128)S(1)}, f32[2]{0:T(128)}, u32[]{:S(2)}) copy-start(f32[2]{0:T(128)} %param.27) | copy-start | bytes 28
  35.5 8.3 %copy-start.8 = (f32[2]{0:T(128)S(1)}, f32[2]{0:T(128)}, u32[]{:S(2)}) copy-start(f32[2]{0:T(128)} %param.28) | copy-start | bytes 28
  44.4 2.1 collective-permute-start
  210.4 371.2 %copy-start.6 = (f32[128]{0:T(128)S(1)}, f32[128]{0:T(128)}, u32[]{:S(2)}) copy-start(f32[128]{0:T(128)} %param.30) | copy-start | bytes 1540
Sparse Core Ops, SparseCore 0:
  48.2 382.0 all-gather.3
where the time goes:
time: 607 us; the launch traced here: 603 us
  waiting for transfers between devices  225 us (37%)
  blocking collectives  171 us (28%)
  other arithmetic  137 us (23%)
  local copies, waits for them, and re-layouts  24.8 us (4%)
  starting transfers between devices  19 us (3%)
  between operations  13.7 us (2%)
  matrix products  7.82 us (1%)
    all_gather x1, waiting for transfers between devices, carried_in(): everything = jax.tree.map(lambda part: lax.all_gather(part, axis), array)  218 us
    all_gather x1, blocking collectives, carried_in(): everything = jax.tree.map(lambda part: lax.all_gather(part, axis), array)  161 us
    select_n x128, other arithmetic, step(): return jax.tree.map(lambda a, b: jnp.where(reached, a, b), new, before)  134 us
    all_to_all x1, starting transfers between devices, from_everyone(): lax.all_to_all(jnp.broadcast_to(array[None], (length, *array.shape)), axi...  17.7 us
    mul x256, local copies, waits for them, and re-layouts, combine(): latter[0][:, :, None, None] * preceding_portion[1] + latter[1]  12.9 us
  transfers between devices with their start and end apart: 3, of which 3 were waited for; matrix products, arithmetic and copies ran while one was open for 2% of the time, Pallas kernels for 0%

commit v1 on v0

--- a/solution.py
+++ b/solution.py
@@ -1,6 +1,10 @@
+import functools
+
 import jax
 import jax.numpy as jnp
 from jax import lax
+from jax.experimental import pallas as pl
+from jax.experimental.pallas import tpu as pltpu
 from jax.sharding import PartitionSpec as P
 
 HEAD_TOTAL = 16
@@ -38,21 +42,146 @@
     return lax.ppermute(array, axis, pairs)
 
 
-def carried_in(array, axis, combine, identity):
-    length, place = (lax.axis_size(axis), lax.axis_index(axis))
-    everything = jax.tree.map(lambda part: lax.all_gather(part, axis), array)
-    start = jax.tree.map(
-        lambda part, zero: jnp.broadcast_to(jnp.asarray(zero, part.dtype), part.shape),
-        array,
-        identity,
-    )
-
-    def step(k, before):
-        reached = k < place
-        new = combine(before, jax.tree.map(lambda part: part[k], everything))
-        return jax.tree.map(lambda a, b: jnp.where(reached, a, b), new, before)
-
-    return lax.fori_loop(0, length, step, start)
+MEMBERS = 16
+MESH = pl.DeviceIdType.MESH
+
+
+def scan_kernel(
+    blocks, state_ref, logs_ref, out_ref,
+    chunk_send, chunk_recv, log_recv, part_sums, part_logs,
+    total_send, total_log, total_recv, total_log_recv, back_send,
+    sem_c, sem_l, sem_t, sem_tl, sem_b,
+):
+    sp = lax.axis_index("sp")
+    block, me = sp // MEMBERS, sp % MEMBERS
+
+    def remote(source, target, sems, slot_here, slot_there, device):
+        return pltpu.make_async_remote_copy(
+            src_ref=source,
+            dst_ref=target,
+            send_sem=sems.at[0, slot_here],
+            recv_sem=sems.at[1, slot_there],
+            device_id={"sp": device},
+            device_id_type=MESH,
+        )
+
+    for k in range(blocks - 1):
+        total_recv[k] = jnp.zeros((16, 128), jnp.bfloat16)
+        total_log_recv[k] = jnp.zeros((1, 128), jnp.float32)
+    for c in range(MEMBERS):
+        chunk_send[c] = state_ref[c * 16 : (c + 1) * 16, :].astype(jnp.bfloat16)
+
+    barrier = pltpu.get_barrier_semaphore()
+    for k in range(1, MEMBERS):
+        pl.semaphore_signal(
+            barrier, inc=1, device_id={"sp": block * MEMBERS + (me + k) % MEMBERS},
+            device_id_type=MESH,
+        )
+    for k in range(1, blocks):
+        pl.semaphore_signal(
+            barrier, inc=1, device_id={"sp": ((block + k) % blocks) * MEMBERS + me},
+            device_id_type=MESH,
+        )
+    pl.semaphore_wait(barrier, MEMBERS + blocks - 2)
+
+    sends = []
+    for k in range(1, MEMBERS):
+        peer = (me + k) % MEMBERS
+        device = block * MEMBERS + peer
+        one = remote(logs_ref.at[peer // 4], log_recv.at[me], sem_l, peer, me, device)
+        one.start()
+        two = remote(chunk_send.at[peer], chunk_recv.at[me], sem_c, peer, me, device)
+        two.start()
+        sends += [one, two]
+    chunk_recv[me] = chunk_send[me]
+    log_recv[me] = logs_ref[me // 4]
+    for k in range(1, MEMBERS):
+        peer = (me + k) % MEMBERS
+        device = block * MEMBERS + peer
+        remote(logs_ref.at[0], log_recv.at[peer], sem_l, me, peer, device).wait_recv()
+        remote(chunk_send.at[0], chunk_recv.at[peer], sem_c, me, peer, device).wait_recv()
+
+    running = jnp.zeros((16, 128), jnp.float32)
+    log_sum = jnp.zeros((1, 128), jnp.float32)
+    for m in range(MEMBERS):
+        part_sums[m] = running
+        part_logs[m] = log_sum
+        here = log_recv[m]
+        running = jnp.exp(here) * running + chunk_recv[m].astype(jnp.float32)
+        log_sum = log_sum + here
+    total_send[...] = running.astype(jnp.bfloat16)
+    total_log[...] = log_sum
+
+    def far(k, device):
+        return (
+            remote(total_log, total_log_recv.at[k - 1], sem_tl, k - 1, k - 1, device),
+            remote(total_send, total_recv.at[k - 1], sem_t, k - 1, k - 1, device),
+        )
+
+    for k in range(1, blocks):
+        @pl.when(block + k < blocks)
+        def _():
+            for copy in far(k, sp + k * MEMBERS):
+                copy.start()
+    for k in range(1, blocks):
+        @pl.when(block >= k)
+        def _():
+            for copy in far(k, sp - k * MEMBERS):
+                copy.wait_recv()
+    incoming = jnp.zeros((16, 128), jnp.float32)
+    for k in range(blocks - 1, 0, -1):
+        incoming = jnp.exp(total_log_recv[k - 1]) * incoming + total_recv[k - 1].astype(jnp.float32)
+    for m in range(MEMBERS):
+        back_send[m] = (part_sums[m] + jnp.exp(part_logs[m]) * incoming).astype(jnp.bfloat16)
+    for k in range(1, MEMBERS):
+        peer = (me + k) % MEMBERS
+        copy = remote(
+            back_send.at[peer], out_ref.at[me], sem_b, peer, me, block * MEMBERS + peer
+        )
+        copy.start()
+        sends.append(copy)
+    out_ref[me] = back_send[me]
+    for k in range(1, MEMBERS):
+        peer = (me + k) % MEMBERS
+        remote(
+            back_send.at[0], out_ref.at[peer], sem_b, me, peer, block * MEMBERS + peer
+        ).wait_recv()
+    for copy in sends:
+        copy.wait_send()
+    for k in range(1, blocks):
+        @pl.when(block + k < blocks)
+        def _():
+            for copy in far(k, sp + k * MEMBERS):
+                copy.wait_send()
+
+
+def states_before(state, logs):
+    blocks = lax.axis_size("sp") // MEMBERS
+    vmem = pl.BlockSpec(memory_space=pltpu.VMEM)
+    return pl.pallas_call(
+        functools.partial(scan_kernel, blocks),
+        out_shape=jax.ShapeDtypeStruct((MEMBERS, 16, 128), jnp.bfloat16),
+        in_specs=[vmem, vmem],
+        out_specs=vmem,
+        scratch_shapes=[
+            pltpu.VMEM((MEMBERS, 16, 128), jnp.bfloat16),
+            pltpu.VMEM((MEMBERS, 16, 128), jnp.bfloat16),
+            pltpu.VMEM((MEMBERS, 1, 128), jnp.float32),
+            pltpu.VMEM((MEMBERS, 16, 128), jnp.float32),
+            pltpu.VMEM((MEMBERS, 1, 128), jnp.float32),
+            pltpu.VMEM((16, 128), jnp.bfloat16),
+            pltpu.VMEM((1, 128), jnp.float32),
+            pltpu.VMEM((blocks - 1, 16, 128), jnp.bfloat16),
+            pltpu.VMEM((blocks - 1, 1, 128), jnp.float32),
+            pltpu.VMEM((MEMBERS, 16, 128), jnp.bfloat16),
+            pltpu.SemaphoreType.DMA((2, MEMBERS)),
+            pltpu.SemaphoreType.DMA((2, MEMBERS)),
+            pltpu.SemaphoreType.DMA((2, blocks)),
+            pltpu.SemaphoreType.DMA((2, blocks)),
+            pltpu.SemaphoreType.DMA((2, MEMBERS)),
+        ],
+        compiler_params=pltpu.CompilerParams(collective_id=0, has_side_effects=True),
+    )(state, logs)
 
 
 def rms_rows(values, gain_row):
@@ -93,34 +222,20 @@
     )
     tail_weight = jnp.exp(inside_block[:, :, -1:, :] - inside_block)
     block_states = jnp.einsum(
-        "sblhn,sblhp->sbhpn", key_heads, x_blocks * tail_weight[..., None], precision=PRECISE
+        "sblhn,sblhp->sbnhp", key_heads, x_blocks * tail_weight[..., None], precision=PRECISE
     )
     block_totals = inside_block[:, :, -1, :]
-    running = jnp.zeros((seq_count, heads_here, HEAD_DIM, STATE), jnp.float32)
-    entering = [running]
-    running = jnp.exp(block_totals[:, 0])[:, :, None, None] * running + block_states[:, 0]
-    entering_states = jnp.stack(entering, axis=1)
-    forwarded_portion = jnp.einsum(
-        "sblhn,sbhpn->sblhp", query_heads, entering_states, precision=PRECISE
-    )
-    forwarded_portion = forwarded_portion * jnp.exp(inside_block)[..., None]
-    local_out = (inner_part + forwarded_portion).reshape(seq_count, seg_len, heads_here, HEAD_DIM)
-    decay_total = jnp.exp(jnp.sum(block_totals, axis=1))
+    local_out = inner_part.reshape(seq_count, seg_len, heads_here, HEAD_DIM)
+    logs = jnp.repeat(jnp.sum(block_totals, axis=1), HEAD_DIM, axis=1)
+    running = block_states.reshape(seq_count * STATE, heads_here * HEAD_DIM)
     prefix_log = jnp.cumsum(log_decay, axis=1)
-    return (local_out, decay_total, running, prefix_log)
+    return (local_out, logs[:, None, :], running, prefix_log)
 
 
 def read_in(local_out, readout_vectors, prefix_log, incoming):
     query_heads = jnp.repeat(readout_vectors, HEAD_TOTAL // GROUPS, axis=2)
-    carried = jnp.einsum("slhn,shpn->slhp", query_heads, incoming, precision=PRECISE)
+    carried = jnp.einsum("slhn,snhp->slhp", query_heads, incoming, precision=PRECISE)
     return local_out + carried * jnp.exp(prefix_log)[..., None]
-
-
-def combine(preceding_portion, latter):
-    return (
-        preceding_portion[0] * latter[0],
-        latter[0][:, :, None, None] * preceding_portion[1] + latter[1],
-    )
 
 
 def body(
@@ -174,16 +289,12 @@
     step_size = jax.nn.softplus(own_steps.astype(jnp.float32) + step_bias)
     log_decay = -step_size * decay_rate + jnp.transpose(decay_extra, (0, 2, 1))
     scaled_x = conv_values * step_size[..., None]
-    local_out, decay_total, final_state, prefix_log = local_pass(
+    local_out, logs, final_state, prefix_log = local_pass(
         scaled_x, keys_b, readout_vectors, log_decay
     )
-    incoming = carried_in(
-        (decay_total, final_state),
-        "sp",
-        combine,
-        (jnp.ones_like(decay_total), jnp.zeros_like(final_state)),
-    )
-    blended_heads = read_in(local_out, readout_vectors, prefix_log, incoming[1])
+    incoming = states_before(final_state, logs)
+    incoming = incoming.reshape(seq_count, STATE, heads_here, HEAD_DIM).astype(jnp.float32)
+    blended_heads = read_in(local_out, readout_vectors, prefix_log, incoming)
     gated_rows = blended_heads.reshape(seq_count, seg_len, inner_here) * jax.nn.silu(
         gate_in.astype(jnp.float32)
     )

time: 607 us -> 93.3 us (0.15)
  waiting for transfers between devices: 225 us -> 6.83 us
  blocking collectives: 171 us -> 11.5 us
  other arithmetic: 137 us -> 3.03 us
  Pallas kernels: 0 us -> 32.2 us
  between operations: 13.7 us -> 0.32 us
  local copies, waits for them, and re-layouts: 24.8 us -> 13.5 us
    all_gather x1 -> x0, waiting for transfers between devices: 218 us -> none  [carried_in(): everything = jax.tree.map(lambda part: lax.all_gather(part, axis), array)]
    all_gather x1 -> x0, blocking collectives: 161 us -> none  [carried_in(): everything = jax.tree.map(lambda part: lax.all_gather(part, axis), array)]
    select_n x128 -> x0, other arithmetic: 134 us -> none  [step(): return jax.tree.map(lambda a, b: jnp.where(reached, a, b), new, before)]
    pallas_call x0 -> x1, Pallas kernels: none -> 32.2 us  [states_before(): pl.pallas_call(functools.partial(scan_kernel, blocks), out_shape=jax.Shap...]
    mul x257 -> x0, local copies, waits for them, and re-layouts: 13 us -> none  [the longest x256 12.9 us: combine(): latter[0][:, :, None, None] * preceding_portion[1] + latter[1]]
  transfers between devices with their start and end apart: 3 -> 2, of which waited for: 3 -> 1; matrix products, arithmetic and copies ran while one was open for 2% -> 10% of each run, Pallas kernels for 0% -> 0%
where the time goes in v1:
time: 93.3 us; the launch traced here: 92.8 us
  Pallas kernels  32.2 us (35%)
  starting transfers between devices  19 us (20%)
  local copies, waits for them, and re-layouts  13.5 us (14%)
  blocking collectives  11.5 us (12%)
  waiting for transfers between devices  6.83 us (7%)
  matrix products  6.4 us (7%)
  other arithmetic  3.03 us (3%)
    pallas_call x1, Pallas kernels, states_before(): pl.pallas_call(functools.partial(scan_kernel, blocks), out_shape=jax.Shap...  32.2 us
    all_to_all x1, starting transfers between devices, from_everyone(): lax.all_to_all(jnp.broadcast_to(array[None], (length, *array.shape)), axi...  17.7 us
    all_to_all x1, blocking collectives, body(): lax.all_to_all(normed_out, 'tp', split_axis=1, concat_axis=2, tiled=True)  11.5 us
    all_to_all x1, waiting for transfers between devices, from_everyone(): lax.all_to_all(jnp.broadcast_to(array[None], (length, *array.shape)), axi...  6.83 us
    unnamed x22, local copies, waits for them, and re-layouts  4.12 us
    concatenate x1, local copies, waits for them, and re-layouts, body(): jnp.concatenate([gate_weight, input_weight, key_weight, query_weight, ste...  4.01 us
    dot_general x1, matrix products, body(): jnp.dot(token_rows.reshape(token_rows.shape[0] * token_rows.shape[1], tok...  3.67 us
  transfers between devices with their start and end apart: 2, of which 1 were waited for; matrix products, arithmetic and copies ran while one was open for 10% of the time, Pallas kernels for 0%

profile of v1, /device:TPU:1, one launch (start us, length us, event | category | flops | bytes accessed | tf_op | source)
XLA Modules:
  0.0 92.8 jit_solution(2816146704625476844)
XLA Ops:
  0.0 1.1 %fusion.3 = f32[4,8]{1,0:T(4,128)S(1)} fusion(bf16[4,8,2048]{2,1,0:T(8,128)(2,1)} %param.15), kind=kLoop, calls=%fused_computation.11 | loop fusion | flops 196576 | bytes 131200 | tf_op jit(solution)/shard_map/reduce_sum | solution.py:188
  1.1 1.0 %fusion.5 = bf16[4,8,2048]{2,1,0:T(8,128)(2,1)S(1)} fusion(bf16[4,8,2048]{2,1,0:T(8,128)(2,1)} %param.15, f32[2048]{0:T(1024)} %param.16, f32[4,8]{1,0:T(4,128)S(1)} %add_rsqrt_fusion.1), kind=kLoop, calls=%fused_computation.13 | loop fusion | flops 262144 | bytes 270464 | tf_op jit(solution)/shard_map/convert_element_type | solution.py:258
  2.1 1.1 %broadcast_in_dim.24 = bf16[8,4,8,2048]{3,2,1,0:T(8,128)(2,1)} broadcast(bf16[4,8,2048]{2,1,0:T(8,128)(2,1)S(1)} %fusion.5), dimensions={1,2,3} | broadcast | bytes 1179648 | tf_op jit(solution)/shard_map/broadcast_in_dim | solution.py:31
  3.2 17.7 %all-to-all-start = ((bf16[8,4,8,2048]{3,2,1,0:T(8,128)(2,1)}), bf16[8,4,8,2048]{3,2,1,0:T(8,128)(2,1)S(1)}, u32[]{:S(2)}, u32[]{:S(2)}) async-start(bf16[8,4,8,2048]{3,2,1,0:T(8,128)(2,1)} %broadcast_in_dim.24), calls=%async_computation | async-start | bytes 2097152 | tf_op jit(solution)/shard_map/all_to_all | solution.py:30
  20.9 2.0 %copy.78 = bf16[2048,64]{1,0:T(8,128)(2,1)} copy(bf16[2048,64]{0,1:T(8,128)(2,1)} %param.19) | data formatting | bytes 524288 | tf_op args[4]
  22.9 1.0 %copy.79 = bf16[2048,64]{1,0:T(8,128)(2,1)} copy(bf16[2048,64]{0,1:T(8,128)(2,1)S(1)} %copy-done) | data formatting | bytes 524288 | tf_op args[5]
  23.9 1.0 %copy.80 = bf16[2048,16]{1,0:T(8,128)(2,1)} copy(bf16[2048,16]{0,1:T(8,128)(2,1)S(1)} %copy-done.1) | data formatting | bytes 131072 | tf_op args[6]
  24.9 4.0 %concatenate.9 = bf16[2048,400]{1,0:T(8,128)(2,1)S(1)} concatenate(bf16[2048,128]{1,0:T(8,128)(2,1)} %param.17, bf16[2048,128]{1,0:T(8,128)(2,1)} %param.18, bf16[2048,64]{1,0:T(8,128)(2,1)} %copy.78, bf16[2048,64]{1,0:T(8,128)(2,1)} %copy.79, bf16[2048,16]{1,0:T(8,128)(2,1)} %copy.80), dimensions={1} | concatenate | bytes 3276800 | tf_op jit(solution)/shard_map/concatenate | solution.py:259
  28.9 0.0 copy-start.7
  28.9 0.0 copy-start.8
  29.0 0.1 pad_maximum_fusion
  29.1 6.8 %all-to-all-done = bf16[8,4,8,2048]{3,2,1,0:T(8,128)(2,1)S(1)} async-done(((bf16[8,4,8,2048]{3,2,1,0:T(8,128)(2,1)}), bf16[8,4,8,2048]{3,2,1,0:T(8,128)(2,1)S(1)}, u32[]{:S(2)}, u32[]{:S(2)}) %all-to-all-start) | async-done | bytes 1048608 | tf_op jit(solution)/shard_map/all_to_all | solution.py:30
  35.9 0.1 copy.77
  36.0 0.9 convolution_convert_fusion.1
  36.9 0.1 copy.81
  37.1 0.1 constant_dynamic-slice_fusion
  37.1 0.1 copy.103
  37.3 0.1 compare_select_fusion
  37.4 0.1 copy.87
  37.5 0.1 reduce_window_sum.22
  37.6 0.1 copy.90
  37.7 0.1 copy.91
  37.8 1.3 %collective-permute-start = (bf16[4,3,256]{2,1,0:T(4,128)(2,1)S(1)}, bf16[4,3,256]{2,1,0:T(4,128)(2,1)S(1)}, u32[]{:S(2)}, u32[]{:S(2)}) collective-permute-start(bf16[4,3,256]{2,1,0:T(4,128)(2,1)S(1)} %slice.66), channel_id=1, source_target_pairs={{0,8},{8,16},{16,24},{24,32},{32,40},{40,48},{48,56},{56,64},{64,7... | collective-permute-start | bytes 18440 | tf_op jit(solution)/shard_map/ppermute | solution.py:42
  39.2 0.1 copy.96
  39.3 0.1 copy.92
  39.4 0.1 broadcast_in_dim.27
  39.5 0.7 broadcast_in_dim_reshape.4.logs_ref
  40.2 0.1 copy.88
  40.2 0.1 reduce_window_sum.23
  40.4 0.1 copy.97
  40.6 0.2 divide_multiply_fusion
  40.8 0.1 fusion.37
  40.9 0.4 convolution_bitcast_fusion.3
  41.3 0.1 copy.101
  41.4 0.4 convolution_bitcast_fusion.1
  41.8 0.2 copy.93
  42.0 0.8 reshape.144.state_ref
  42.8 32.2 %shard_map.145 = bf16[16,16,128]{2,1,0:T(8,128)(2,1)} custom-call(f32[256,128]{1,0:T(8,128)} %reshape.144.state_ref, f32[4,1,128]{2,1,0:T(1,128)} %broadcast_in_dim_reshape.4.logs_ref), custom_call_target="tpu_custom_call" | custom-call | tf_op jit(solution)/shard_map/pallas_call | solution.py:161
  75.0 0.9 %reshape.145 = bf16[4,64,2,64]{3,2,1,0:T(2,128)(2,1)S(1)} reshape(bf16[16,16,128]{2,1,0:T(8,128)(2,1)} %shard_map.145) | data formatting | bytes 131072 | tf_op jit(solution)/shard_map/reshape | solution.py:296
  76.0 0.1 copy.85
  76.1 0.7 convolution_bitcast_fusion.2
  76.7 0.4 fusion.2
  77.1 0.1 copy.98
  77.2 0.1 multiply_reduce_fusion
  77.4 0.1 multiply_convert_fusion
  77.5 0.1 copy.99
  77.6 11.5 %all_to_all.20 = bf16[4,64,128]{2,0,1:T(4,128)(2,1)S(1)} all-to-all(bf16[4,64,128]{2,0,1:T(4,128)(2,1)S(1)} %copy.99), channel_id=1, replica_groups=mesh['sp'=128,'tp'=8] {'tp'}, dimensions={1} | all-to-all | bytes 131072 | tf_op jit(solution)/shard_map/all_to_all | solution.py:308
  89.1 3.7 %fusion = bf16[4,8,2048]{2,1,0:T(8,128)(2,1)} fusion(bf16[1024,2048]{1,0:T(8,128)(2,1)} %param.29, bf16[4,64,128]{2,0,1:T(4,128)(2,1)S(1)} %all_to_all.20), kind=kOutput, calls=%fused_computation.1 | convolution fusion | flops 134283264 | bytes 4390912 | tf_op jit(solution)/shard_map/dot_general | solution.py:309
  (30 shorter events, 0.2 us)
Async XLA Ops:
  0.0 22.9 %copy-start = (bf16[2048,64]{0,1:T(8,128)(2,1)S(1)}, bf16[2048,64]{0,1:T(8,128)(2,1)}, u32[]{:S(2)}) copy-start(bf16[2048,64]{0,1:T(8,128)(2,1)} %param.20) | copy-start | bytes 786436
  0.0 23.9 %copy-start.1 = (bf16[2048,16]{0,1:T(8,128)(2,1)S(1)}, bf16[2048,16]{0,1:T(8,128)(2,1)}, u32[]{:S(2)}) copy-start(bf16[2048,16]{0,1:T(8,128)(2,1)} %param.21) | copy-start | bytes 196612
  3.2 25.7 %copy-start.3 = (f32[4,64]{1,0:T(4,128)S(1)}, f32[4,64]{1,0:T(4,128)}, u32[]{:S(2)}) copy-start(f32[4,64]{1,0:T(4,128)} %param.24) | copy-start | bytes 3076
  3.2 25.7 %copy-start.4 = (f32[4,64]{1,0:T(4,128)S(1)}, f32[4,64]{1,0:T(4,128)}, u32[]{:S(2)}) copy-start(f32[4,64]{1,0:T(4,128)} %param.23) | copy-start | bytes 3076
  3.2 25.7 %copy-start.5 = (f32[4,128]{1,0:T(4,128)S(1)}, f32[4,128]{1,0:T(4,128)}, u32[]{:S(2)}) copy-start(f32[4,128]{1,0:T(4,128)} %param.22) | copy-start | bytes 6148
  3.2 32.7 %all-to-all-start = ((bf16[8,4,8,2048]{3,2,1,0:T(8,128)(2,1)}), bf16[8,4,8,2048]{3,2,1,0:T(8,128)(2,1)S(1)}, u32[]{:S(2)}, u32[]{:S(2)}) async-start(bf16[8,4,8,2048]{3,2,1,0:T(8,128)(2,1)} %broadcast_in_dim.24), calls=%async_computation | async-start | bytes 2097152 | tf_op jit(solution)/shard_map/all_to_all | solution.py:30
  28.9 8.3 %copy-start.2 = (f32[4,2,64]{2,1,0:T(2,128)S(1)}, f32[4,2,64]{2,1,0:T(2,128)}, u32[]{:S(2)}) copy-start(f32[4,2,64]{2,1,0:T(2,128)} %param.27) | copy-start | bytes 6148
  28.9 8.3 %copy-start.7 = (f32[2]{0:T(128)S(1)}, f32[2]{0:T(128)}, u32[]{:S(2)}) copy-start(f32[2]{0:T(128)} %param.25) | copy-start | bytes 28
  28.9 8.3 %copy-start.8 = (f32[2]{0:T(128)S(1)}, f32[2]{0:T(128)}, u32[]{:S(2)}) copy-start(f32[2]{0:T(128)} %param.26) | copy-start | bytes 28
  37.8 2.7 %collective-permute-start = (bf16[4,3,256]{2,1,0:T(4,128)(2,1)S(1)}, bf16[4,3,256]{2,1,0:T(4,128)(2,1)S(1)}, u32[]{:S(2)}, u32[]{:S(2)}) collective-permute-start(bf16[4,3,256]{2,1,0:T(4,128)(2,1)S(1)} %slice.66), channel_id=1, source_target_pairs={{0,8},{8,16},{16,24},{24,32},{32,40},{40,48},{48,56},{56,64},{64,7... | collective-permute-start | bytes 18440 | tf_op jit(solution)/shard_map/ppermute | solution.py:42
  40.2 37.2 %copy-start.6 = (f32[128]{0:T(128)S(1)}, f32[128]{0:T(128)}, u32[]{:S(2)}) copy-start(f32[128]{0:T(128)} %param.28) | copy-start | bytes 1540

commit v2 on v1

v2 whole, which is shorter than its diff:
```python
import functools

import jax
import jax.numpy as jnp
from jax import lax
from jax.experimental import pallas as pl
from jax.experimental.pallas import tpu as pltpu
from jax.sharding import PartitionSpec as P

STATE = 64
NORM_EPS = 1e-06
PRECISE = lax.Precision.HIGHEST
MEMBERS = 16
MESH = pl.DeviceIdType.MESH
F32 = jnp.float32
BF16 = jnp.bfloat16


def rounded(values):
    return values.astype(BF16).astype(F32)


def two_parts(values):
    high = values.astype(BF16)
    return high, (values - high.astype(F32)).astype(BF16)


def three_parts(values):
    high = values.astype(BF16)
    rest = values - high.astype(F32)
    middle = rest.astype(BF16)
    return high, middle, (rest - middle.astype(F32)).astype(BF16)


def silu(values):
    return values / (1.0 + jnp.exp(-values))


def softplus(values):
    return jnp.maximum(values, 0.0) + jnp.log1p(jnp.exp(-jnp.abs(values)))


def dot(a, b, contract=((1,), (0,)), precision=None):
    return lax.dot_general(
        a, b, (contract, ((), ())), precision=precision, preferred_element_type=F32
    )


def mixer_kernel(
    places, seqs,
    tokens_ref, gain_ref, gate_ref, input_ref, key_ref, query_ref, step_ref,
    conv_x_ref, conv_k_ref, conv_q_ref, bias_ref, rate_ref, extra_ref, out_gain_ref, out_w_ref,
    out_ref,
    tok, w_gi, w_kq, w_step, w_out, rows_in,
    gate_s, x_pad, kq_pad, step_s, extra_s,
    xs_s, kq_s, cum_s, inner_s, query_s,
    rim_send, rim_recv,
    chunk_send, chunk_recv, log_send, log_recv, part_sums, part_logs,
    total_send, total_log, total_recv, total_log_recv, back_send, back_recv,
    mix_send, mix_recv,
    sem_load, sem_gs, sem_gr, sem_rim, sem_c, sem_l, sem_t, sem_tl, sem_b, sem_m,
):
    blocks = places // MEMBERS
    sp, tp = lax.axis_index("sp"), lax.axis_index("tp")
    block, me = sp // MEMBERS, sp % MEMBERS
    chip, core = tp // 2, tp % 2
    ahead, behind = ((chip + 1) % 4) * 2 + core, ((chip + 3) % 4) * 2 + core
    partner = chip * 2 + 1 - core

    def load(k, source, target):
        copy = pltpu.make_async_copy(source, target, sem_load.at[k])
        copy.start()
        return copy

    tok_load = load(0, tokens_ref, tok)
    weight_loads = [
        load(1, gate_ref, w_gi.at[:, 0:128]),
        load(2, input_ref, w_gi.at[:, 128:256]),
        load(3, key_ref, w_kq.at[0:64, :]),
        load(4, query_ref, w_kq.at[64:128, :]),
    ]
    step_load = load(5, step_ref, w_step)
    out_load = load(6, out_w_ref, w_out)

    def remote(source, target, send_sem, recv_sem, **device):
        return pltpu.make_async_remote_copy(
            src_ref=source, dst_ref=target, send_sem=send_sem, recv_sem=recv_sem,
            device_id=device, device_id_type=MESH,
        )

    def pair(source, target, sems, here, there, device):
        return remote(source, target, sems.at[0, here], sems.at[1, there], sp=device)

    for k in range(blocks - 1):
        total_recv[k] = jnp.zeros((16, 128), BF16)
        total_log_recv[k] = jnp.zeros((1, 128), F32)

    @pl.when(sp == 0)
    def _():
        rim_recv[...] = jnp.zeros_like(rim_recv)

    barrier = pltpu.get_barrier_semaphore()

    def greet(**device):
        pl.semaphore_signal(barrier, inc=1, device_id=device, device_id_type=MESH)

    for k in range(1, 8):
        greet(tp=(tp + k) % 8)
    for k in range(1, MEMBERS):
        greet(sp=block * MEMBERS + (me + k) % MEMBERS)
    for k in range(1, blocks):
        greet(sp=((block + k) % blocks) * MEMBERS + me)
    greet(sp=(sp + 1) % places)
    greet(sp=(sp + places - 1) % places)

    tok_load.wait()
    values = tok[...].astype(F32).reshape(seqs * 8, tok.shape[2])
    mean_sq = jnp.mean(values * values, axis=-1, keepdims=True)
    rows_in[0] = (values * lax.rsqrt(mean_sq + NORM_EPS) * gain_ref[...]).astype(BF16)

    pl.semaphore_wait(barrier, 7 + MEMBERS - 1 + blocks - 1 + 2)

    gather_sends = []

    def pass_on(k, slot, half, to_slot, device):
        part = pl.ds(half * 16, 16)
        copy = remote(
            rows_in.at[slot, part], rows_in.at[to_slot, part],
            sem_gs.at[k], sem_gr.at[to_slot, half], tp=device,
        )
        copy.start()
        gather_sends.append(copy)

    def arrived(slot, half):
        part = pl.ds(half * 16, 16)
        remote(
            rows_in.at[slot, part], rows_in.at[slot, part],
            sem_gs.at[0], sem_gr.at[slot, half], tp=partner,
        ).wait_recv()

    pass_on(0, 0, 0, 4, ahead)
    pass_on(1, 0, 1, 2, behind)
    pass_on(2, 0, 1, 4, ahead)
    pass_on(3, 0, 0, 2, behind)
    pass_on(4, 0, 0, 1, partner)
    pass_on(5, 0, 1, 1, partner)

    row = lax.broadcasted_iota(jnp.int32, (64, 128), 0)
    lane = lax.broadcasted_iota(jnp.int32, (64, 128), 1)
    inside = lane % 64
    diagonal = row == inside
    causal = row >= inside
    first_head = lane < 64
    lane_row = lax.broadcasted_iota(jnp.int32, (1, 128), 1)
    bias_row = jnp.where(lane_row < 64, bias_ref[0], bias_ref[1])
    rate_row = jnp.where(lane_row < 64, rate_ref[0], rate_ref[1])

    step_load.wait()
    pick_row = lax.broadcasted_iota(jnp.int32, (128, 16), 0) // 64 + 2 * tp
    pick = (pick_row == lax.broadcasted_iota(jnp.int32, (128, 16), 1)).astype(F32).astype(BF16)
    w_kq[128:256, :] = dot(pick, w_step[...]).astype(BF16)
    same_head = (
        lax.broadcasted_iota(jnp.int32, (128, 128), 0) // 64
        == lax.broadcasted_iota(jnp.int32, (128, 128), 1) // 64
    ).astype(F32)
    for s in range(seqs):
        extra_row = jnp.concatenate([extra_ref[s, 0:1, :], extra_ref[s, 1:2, :]], axis=1)
        extra_s[s] = dot(jnp.where(diagonal, extra_row, 0.0), same_head, precision=PRECISE)
    for copy in weight_loads:
        copy.wait()

    arrived(4, 0)
    pass_on(6, 4, 0, 6, ahead)
    pass_on(7, 4, 0, 5, partner)
    arrived(2, 1)
    pass_on(8, 2, 1, 6, behind)
    pass_on(9, 2, 1, 3, partner)
    arrived(4, 1)
    pass_on(10, 4, 1, 5, partner)
    arrived(2, 0)
    pass_on(11, 2, 0, 3, partner)
    arrived(6, 0)
    pass_on(12, 6, 0, 7, partner)
    arrived(6, 1)
    pass_on(13, 6, 1, 7, partner)
    for slot in (1, 3, 5):
        arrived(slot, 0)
        arrived(slot, 1)

    position = [
        ((chip + away) % 4) * 2 + (core if same else 1 - core)
        for away in (0, 1, 3, 2)
        for same in (True, False)
    ]

    def project(first, count):
        rows = rows_in[first : first + count].reshape(count * 32, rows_in.shape[2])
        gate_x = rounded(dot(rows, w_gi[...]))
        kq_step = rounded(dot(rows, w_kq[...], ((1,), (1,))))
        for i in range(count):
            at = pl.multiple_of(position[first + i] * 8, 8)
            for s in range(seqs):
                part = slice(i * 32 + s * 8, i * 32 + s * 8 + 8)
                gate_s[s, pl.ds(at, 8), :] = gate_x[part, 0:128]
                x_pad[s, pl.ds(at + 8, 8), :] = gate_x[part, 128:256]
                kq_pad[s, pl.ds(at + 8, 8), :] = kq_step[part, 0:128]
                step_s[s, pl.ds(at, 8), :] = kq_step[part, 128:256]

    project(0, 6)
    arrived(7, 0)
    arrived(7, 1)
    project(6, 2)

    for i, padded in enumerate((x_pad, kq_pad)):
        tails = [padded[s, 64:72, :] for s in range(seqs)]
        rim_send[i] = jnp.concatenate(tails, axis=0).astype(BF16)

    def rim(device):
        return remote(rim_send, rim_recv, sem_rim.at[0], sem_rim.at[1], sp=device)

    @pl.when(sp + 1 < places)
    def _():
        rim(sp + 1).start()

    triangle = (
        lax.broadcasted_iota(jnp.int32, (64, 192), 0)
        >= lax.broadcasted_iota(jnp.int32, (64, 192), 1) % 64
    ).astype(F32).astype(BF16)
    for s in range(seqs):
        step = softplus(step_s[s] + bias_row)
        step_s[s] = step
        log_decay = extra_s[s] - step * rate_row
        cum = dot(triangle, jnp.concatenate(three_parts(log_decay), axis=0))
        cum_s[s] = cum
        log_send[s] = cum[63:64, :]

    @pl.when(sp > 0)
    def _():
        rim(sp - 1).wait_recv()

    conv_kq = jnp.concatenate([conv_k_ref[...], conv_q_ref[...]], axis=1)
    rim_x, rim_kq = rim_recv[0].astype(F32), rim_recv[1].astype(F32)
    for s in range(seqs):
        x_pad[s, 0:8, :] = rim_x[s * 8 : s * 8 + 8, :]
        kq_pad[s, 0:8, :] = rim_kq[s * 8 : s * 8 + 8, :]
        x_sum = x_pad[s, 5:69, :] * conv_x_ref[0:1, :]
        kq_sum = kq_pad[s, 5:69, :] * conv_kq[0:1, :]
        for k in range(1, 4):
            x_sum = x_sum + x_pad[s, 5 + k : 69 + k, :] * conv_x_ref[k : k + 1, :]
            kq_sum = kq_sum + kq_pad[s, 5 + k : 69 + k, :] * conv_kq[k : k + 1, :]
        scaled = silu(x_sum) * step_s[s]
        kq = silu(kq_sum)
        xs_s[s] = scaled
        kq_s[s] = kq
        cum = cum_s[s]
        x_high, x_low = two_parts(scaled * jnp.exp(cum[63:64, :] - cum))
        k_high, k_low = two_parts(kq[:, 0:64])
        state = dot(
            jnp.concatenate([k_high, k_high, k_low], axis=0),
            jnp.concatenate([x_high, x_low, x_high], axis=0),
            ((0,), (0,)),
        )
        for q in range(4):
            chunk_send[s * 4 + q] = state[q * 16 : q * 16 + 16, :].astype(BF16)

    sends = []
    for k in range(1, MEMBERS):
        peer = (me + k) % MEMBERS
        device = block * MEMBERS + peer
        one = pair(log_send.at[peer // 4], log_recv.at[me], sem_l, peer, me, device)
        one.start()
        two = pair(chunk_send.at[peer], chunk_recv.at[me], sem_c, peer, me, device)
        two.start()
        sends += [one, two]
    chunk_recv[me] = chunk_send[me]
    log_recv[me] = log_send[me // 4]

    for s in range(seqs):
        cum, kq, scaled = cum_s[s], kq_s[s], xs_s[s]
        keys, queries = kq[:, 0:64], kq[:, 64:128]
        query_s[s] = jnp.concatenate(two_parts(queries), axis=1)
        cum_row = jnp.sum(jnp.where(diagonal, cum, 0.0), axis=0, keepdims=True)
        decay = jnp.where(causal, jnp.exp(jnp.where(causal, cum - cum_row, 0.0)), 0.0)
        scores = dot(queries, jnp.concatenate([keys, keys], axis=0), ((1,), (1,)), PRECISE)
        apart = jnp.concatenate(
            [jnp.where(first_head, scaled, 0.0), jnp.where(first_head, 0.0, scaled)], axis=0
        )
        inner_s[s] = dot(scores * decay, apart, precision=PRECISE)
        cum_s[s] = jnp.exp(cum)
        gate_s[s] = silu(gate_s[s])

    for k in range(1, MEMBERS):
        peer = (me + k) % MEMBERS
        device = block * MEMBERS + peer
        pair(log_send.at[0], log_recv.at[peer], sem_l, me, peer, device).wait_recv()
        pair(chunk_send.at[0], chunk_recv.at[peer], sem_c, me, peer, device).wait_recv()

    running = jnp.zeros((16, 128), F32)
    log_sum = jnp.zeros((1, 128), F32)
    for m in range(MEMBERS):
        part_sums[m] = running
        part_logs[m] = log_sum
        here = log_recv[m]
        running = jnp.exp(here) * running + chunk_recv[m].astype(F32)
        log_sum = log_sum + here
    total_send[...] = running.astype(BF16)
    total_log[...] = log_sum

    def far(k, device):
        return (
            pair(total_log, total_log_recv.at[k - 1], sem_tl, k - 1, k - 1, device),
            pair(total_send, total_recv.at[k - 1], sem_t, k - 1, k - 1, device),
        )

    for k in range(1, blocks):
        @pl.when(block + k < blocks)
        def _():
            for copy in far(k, sp + k * MEMBERS):
                copy.start()
    for m in range(MEMBERS):
        part_logs[m] = jnp.exp(part_logs[m])
    out_load.wait()
    for k in range(1, blocks):
        @pl.when(block >= k)
        def _():
            for copy in far(k, sp - k * MEMBERS):
                copy.wait_recv()
    incoming = jnp.zeros((16, 128), F32)
    for k in range(blocks - 1, 0, -1):
        incoming = jnp.exp(total_log_recv[k - 1]) * incoming + total_recv[k - 1].astype(F32)
    for m in range(MEMBERS):
        back_send[m] = (part_sums[m] + part_logs[m] * incoming).astype(BF16)
    for k in range(1, MEMBERS):
        peer = (me + k) % MEMBERS
        copy = pair(
            back_send.at[peer], back_recv.at[me], sem_b, peer, me, block * MEMBERS + peer
        )
        copy.start()
        sends.append(copy)
    back_recv[me] = back_send[me]
    for k in range(1, MEMBERS):
        peer = (me + k) % MEMBERS
        pair(
            back_send.at[0], back_recv.at[peer], sem_b, me, peer, block * MEMBERS + peer
        ).wait_recv()

    mixed = []
    for s in range(seqs):
        state = back_recv[s * 4 : s * 4 + 4].reshape(64, 128)
        carried = dot(query_s[s], jnp.concatenate([state, state], axis=0))
        gated = (inner_s[s] + carried * cum_s[s]) * gate_s[s]
        mean_sq = jnp.mean(gated * gated, axis=-1, keepdims=True)
        mixed.append(gated * lax.rsqrt(mean_sq + NORM_EPS) * out_gain_ref[...])
    for t in range(8):
        mix_send[t] = jnp.concatenate(
            [part[t * 8 : t * 8 + 8, :] for part in mixed], axis=0
        ).astype(BF16)
    for k in range(1, 8):
        peer = (tp + k) % 8
        copy = remote(
            mix_send.at[peer], mix_recv.at[tp], sem_m.at[0, peer], sem_m.at[1, tp], tp=peer
        )
        copy.start()
        sends.append(copy)
    mix_recv[tp] = mix_send[tp]
    for k in range(1, 8):
        peer = (tp + k) % 8
        remote(
            mix_send.at[0], mix_recv.at[peer], sem_m.at[0, tp], sem_m.at[1, peer], tp=peer
        ).wait_recv()
    rows = jnp.concatenate([mix_recv[t] for t in range(8)], axis=1)
    result = dot(rows, w_out[...])
    out_ref[...] = result.reshape(seqs, 8, result.shape[1]).astype(BF16)

    for copy in gather_sends + sends:
        copy.wait_send()

    @pl.when(sp + 1 < places)
    def _():
        rim(sp + 1).wait_send()

    for k in range(1, blocks):
        @pl.when(block + k < blocks)
        def _():
            for copy in far(k, sp + k * MEMBERS):
                copy.wait_send()


def body(
    tokens, in_gain, gate_weight, input_weight, key_weight, query_weight, step_weight,
    conv_input, conv_key, conv_query, step_bias, decay_rate, decay_extra, out_gain, out_weight,
):
    places = lax.axis_size("sp")
    blocks = places // MEMBERS
    seqs, _, width = tokens.shape
    inner = out_weight.shape[0]
    vmem = pl.BlockSpec(memory_space=pltpu.VMEM)
    smem = pl.BlockSpec(memory_space=pltpu.SMEM)
    anywhere = pl.BlockSpec(memory_space=pl.ANY)
    local = (seqs, 64, 128)
    padded = (seqs, 72, 128)
    dma = pltpu.SemaphoreType.DMA
    return pl.pallas_call(
        functools.partial(mixer_kernel, places, seqs),
        out_shape=jax.ShapeDtypeStruct(tokens.shape, BF16),
        in_specs=[
            anywhere, vmem, anywhere, anywhere, anywhere, anywhere, anywhere,
            vmem, vmem, vmem, smem, smem, vmem, vmem, anywhere,
        ],
        out_specs=vmem,
        scratch_shapes=[
            pltpu.VMEM(tokens.shape, BF16),
            pltpu.VMEM((width, 256), BF16),
            pltpu.VMEM((256, width), BF16),
            pltpu.VMEM((16, width), BF16),
            pltpu.VMEM((inner, width), BF16),
            pltpu.VMEM((8, seqs * 8, width), BF16),
            pltpu.VMEM(local, F32),
            pltpu.VMEM(padded, F32),
            pltpu.VMEM(padded, F32),
            pltpu.VMEM(local, F32),
            pltpu.VMEM(local, F32),
            pltpu.VMEM(local, F32),
            pltpu.VMEM(local, F32),
            pltpu.VMEM(local, F32),
            pltpu.VMEM(local, F32),
            pltpu.VMEM(local, BF16),
            pltpu.VMEM((2, seqs * 8, 128), BF16),
            pltpu.VMEM((2, seqs * 8, 128), BF16),
            pltpu.VMEM((MEMBERS, 16, 128), BF16),
            pltpu.VMEM((MEMBERS, 16, 128), BF16),
            pltpu.VMEM((seqs, 1, 128), F32),
            pltpu.VMEM((MEMBERS, 1, 128), F32),
            pltpu.VMEM((MEMBERS, 16, 128), F32),
            pltpu.VMEM((MEMBERS, 1, 128), F32),
            pltpu.VMEM((16, 128), BF16),
            pltpu.VMEM((1, 128), F32),
            pltpu.VMEM((blocks - 1, 16, 128), BF16),
            pltpu.VMEM((blocks - 1, 1, 128), F32),
            pltpu.VMEM((MEMBERS, 16, 128), BF16),
            pltpu.VMEM((MEMBERS, 16, 128), BF16),
            pltpu.VMEM((8, seqs * 8, 128), BF16),
            pltpu.VMEM((8, seqs * 8, 128), BF16),
            dma((7,)),
            dma((14,)),
            dma((8, 2)),
            dma((2,)),
            dma((2, MEMBERS)),
            dma((2, MEMBERS)),
            dma((2, blocks)),
            dma((2, blocks)),
            dma((2, MEMBERS)),
            dma((2, 8)),
        ],
        compiler_params=pltpu.CompilerParams(collective_id=0, has_side_effects=True),
        name="mixer",
    )(
        tokens, in_gain.reshape(1, width), gate_weight, input_weight, key_weight.T,
        query_weight.T, step_weight.T, conv_input, conv_key, conv_query, step_bias, decay_rate,
        decay_extra, out_gain.reshape(1, 128), out_weight,
    )


def solution(mesh):
    placed = (
        P(None, ("sp", "tp"), None),
        P(),
        P(None, "tp"),
        P(None, "tp"),
        P(None, "tp"),
        P(None, "tp"),
        P(),
        P(None, "tp"),
        P(None, "tp"),
        P(None, "tp"),
        P("tp"),
        P("tp"),
        P(None, "tp", "sp"),
        P("tp"),
        P(),
    )
    return jax.shard_map(
        body, mesh=mesh, in_specs=placed, out_specs=P(None, ("sp", "tp"), None), check_vma=False
    )
```

time: 93.3 us -> 64.2 us (0.69)
  Pallas kernels: 32.2 us -> 62.5 us
  starting transfers between devices: 19 us -> 0 us
  local copies, waits for them, and re-layouts: 13.5 us -> 1.57 us
  blocking collectives: 11.5 us -> 0 us
  waiting for transfers between devices: 6.83 us -> 0 us
  matrix products: 6.4 us -> 0 us
  other arithmetic: 3.03 us -> 0 us
    pallas_call x1, Pallas kernels: 32.2 us -> 62.5 us  [body(): pl.pallas_call(functools.partial(mixer_kernel, places, seqs), out_shape=j...]
    all_to_all x1 -> x0, starting transfers between devices: 17.7 us -> none  [from_everyone(): lax.all_to_all(jnp.broadcast_to(array[None], (length, *array.shape)), axi...]
    all_to_all x1 -> x0, blocking collectives: 11.5 us -> none  [body(): lax.all_to_all(normed_out, 'tp', split_axis=1, concat_axis=2, tiled=True)]
    all_to_all x1 -> x0, waiting for transfers between devices: 6.83 us -> none  [from_everyone(): lax.all_to_all(jnp.broadcast_to(array[None], (length, *array.shape)), axi...]
    dot_general x6 -> x0, matrix products: 6.4 us -> none  [the longest x1 3.67 us: body(): jnp.dot(token_rows.reshape(token_rows.shape[0] * token_rows.shape[1], tok...]
    concatenate x1 -> x0, local copies, waits for them, and re-layouts: 4.01 us -> none  [body(): jnp.concatenate([gate_weight, input_weight, key_weight, query_weight, ste...]
    unnamed x22 -> x1, local copies, waits for them, and re-layouts: 4.12 us -> 1.57 us
    reshape x5 -> x0, local copies, waits for them, and re-layouts: 2.14 us -> none  [the longest x1 0.94 us: body(): incoming.reshape(seq_count, STATE, heads_here, HEAD_DIM).astype(jnp.float32)]
  transfers between devices with their start and end apart: 2 -> 0, of which waited for: 1 -> 0; matrix products, arithmetic and copies ran while one was open for 10% -> 0% of each run, Pallas kernels for 0% -> 0%
where the time goes in v2:
time: 64.2 us; the launch traced here: 64 us
  Pallas kernels  62.5 us (97%)
  local copies, waits for them, and re-layouts  1.57 us (2%)
    pallas_call x1, Pallas kernels, body(): pl.pallas_call(functools.partial(mixer_kernel, places, seqs), out_shape=j...  62.5 us
    unnamed x1, local copies, waits for them, and re-layouts  1.57 us

profile of v2, /device:TPU:1, one launch (start us, length us, event | category | flops | bytes accessed | tf_op | source)
XLA Modules:
  0.0 64.0 jit_solution(5307717394437847025)
XLA Ops:
  0.0 62.5 %mixer.1 = bf16[4,8,2048]{2,1,0:T(8,128)(2,1)} custom-call(bf16[4,8,2048]{2,1,0:T(8,128)(2,1)} %tokens_ref.1, f32[1,2048]{1,0:T(1,128)} %bitcast.8, bf16[2048,128]{1,0:T(8,128)(2,1)} %gate_ref.1, bf16[2048,128]{1,0:T(8,128)(2,1)} %input_ref.1, bf16[64,2048]{1,0:T(8,128)(2,1)} %bitcast.5, bf16[64,2048]{1,0:T(8,128)(2,1)} %bitcast.6, ...), custom_call_target="tpu_custom_call" | custom-call | tf_op jit(solution)/shard_map/mixer/pallas_call | solution.py:403
  62.5 1.6 %copy.17 = bf16[4,8,2048]{2,1,0:T(8,128)(2,1)} copy(bf16[4,8,2048]{2,1,0:T(8,128)(2,1)} %mixer.1) | data formatting | bytes 262144

commit v3 on v2

--- a/solution.py
+++ b/solution.py
@@ -58,7 +58,7 @@
     chunk_send, chunk_recv, log_send, log_recv, part_sums, part_logs,
     total_send, total_log, total_recv, total_log_recv, back_send, back_recv,
     mix_send, mix_recv,
-    sem_load, sem_gs, sem_gr, sem_rim, sem_c, sem_l, sem_t, sem_tl, sem_b, sem_m,
+    sem_load, sem_gs, sem_gr, sem_rim, sem_c, sem_l, sem_t, sem_tl, sem_b, sem_m, sem_known,
 ):
     blocks = places // MEMBERS
     sp, tp = lax.axis_index("sp"), lax.axis_index("tp")
@@ -66,6 +66,20 @@
     chip, core = tp // 2, tp % 2
     ahead, behind = ((chip + 1) % 4) * 2 + core, ((chip + 3) % 4) * 2 + core
     partner = chip * 2 + 1 - core
+    place_y = sp % 4
+    row_start = sp - place_y
+
+    def along(chips):
+        return (sp + 4 * chips + places) % places
+
+    def tell(stage):
+        for chips in (2**stage, -(2**stage)):
+            pl.semaphore_signal(
+                sem_known.at[stage], inc=1, device_id={"sp": along(chips)}, device_id_type=MESH
+            )
+
+    def hear(stage):
+        pl.semaphore_wait(sem_known.at[stage], 2)
 
     def load(k, source, target):
         copy = pltpu.make_async_copy(source, target, sem_load.at[k])
@@ -106,19 +120,17 @@
 
     for k in range(1, 8):
         greet(tp=(tp + k) % 8)
-    for k in range(1, MEMBERS):
-        greet(sp=block * MEMBERS + (me + k) % MEMBERS)
-    for k in range(1, blocks):
-        greet(sp=((block + k) % blocks) * MEMBERS + me)
-    greet(sp=(sp + 1) % places)
-    greet(sp=(sp + places - 1) % places)
+    for k in range(1, 4):
+        greet(sp=row_start + (place_y + k) % 4)
+    greet(sp=along(1))
+    greet(sp=along(-1))
 
     tok_load.wait()
     values = tok[...].astype(F32).reshape(seqs * 8, tok.shape[2])
     mean_sq = jnp.mean(values * values, axis=-1, keepdims=True)
     rows_in[0] = (values * lax.rsqrt(mean_sq + NORM_EPS) * gain_ref[...]).astype(BF16)
 
-    pl.semaphore_wait(barrier, 7 + MEMBERS - 1 + blocks - 1 + 2)
+    pl.semaphore_wait(barrier, 7 + 3 + 2)
 
     gather_sends = []
 
@@ -144,6 +156,7 @@
     pass_on(3, 0, 0, 2, behind)
     pass_on(4, 0, 0, 1, partner)
     pass_on(5, 0, 1, 1, partner)
+    tell(0)
 
     row = lax.broadcasted_iota(jnp.int32, (64, 128), 0)
     lane = lax.broadcasted_iota(jnp.int32, (64, 128), 1)
@@ -168,6 +181,8 @@
         extra_s[s] = dot(jnp.where(diagonal, extra_row, 0.0), same_head, precision=PRECISE)
     for copy in weight_loads:
         copy.wait()
+    hear(0)
+    tell(1)
 
     arrived(4, 0)
     pass_on(6, 4, 0, 6, ahead)
@@ -175,6 +190,8 @@
     arrived(2, 1)
     pass_on(8, 2, 1, 6, behind)
     pass_on(9, 2, 1, 3, partner)
+    hear(1)
+    tell(2)
     arrived(4, 1)
     pass_on(10, 4, 1, 5, partner)
     arrived(2, 0)
@@ -183,9 +200,14 @@
     pass_on(12, 6, 0, 7, partner)
     arrived(6, 1)
     pass_on(13, 6, 1, 7, partner)
-    for slot in (1, 3, 5):
-        arrived(slot, 0)
-        arrived(slot, 1)
+    hear(2)
+    tell(3)
+    def partner_rows():
+        for slot in (1, 3, 5):
+            arrived(slot, 0)
+            arrived(slot, 1)
+
+    partner_rows()
 
     position = [
         ((chip + away) % 4) * 2 + (core if same else 1 - core)
@@ -207,8 +229,12 @@
                 step_s[s, pl.ds(at, 8), :] = kq_step[part, 128:256]
 
     project(0, 6)
-    arrived(7, 0)
-    arrived(7, 1)
+
+    def last_rows():
+        arrived(7, 0)
+        arrived(7, 1)
+
+    last_rows()
     project(6, 2)
 
     for i, padded in enumerate((x_pad, kq_pad)):
@@ -234,9 +260,12 @@
         cum_s[s] = cum
         log_send[s] = cum[63:64, :]
 
-    @pl.when(sp > 0)
-    def _():
-        rim(sp - 1).wait_recv()
+    def rim_rows():
+        @pl.when(sp > 0)
+        def _():
+            rim(sp - 1).wait_recv()
+
+    rim_rows()
 
     conv_kq = jnp.concatenate([conv_k_ref[...], conv_q_ref[...]], axis=1)
     rim_x, rim_kq = rim_recv[0].astype(F32), rim_recv[1].astype(F32)
@@ -289,11 +318,14 @@
         cum_s[s] = jnp.exp(cum)
         gate_s[s] = silu(gate_s[s])
 
-    for k in range(1, MEMBERS):
-        peer = (me + k) % MEMBERS
-        device = block * MEMBERS + peer
-        pair(log_send.at[0], log_recv.at[peer], sem_l, me, peer, device).wait_recv()
-        pair(chunk_send.at[0], chunk_recv.at[peer], sem_c, me, peer, device).wait_recv()
+    def chunks_here():
+        for k in range(1, MEMBERS):
+            peer = (me + k) % MEMBERS
+            device = block * MEMBERS + peer
+            pair(log_send.at[0], log_recv.at[peer], sem_l, me, peer, device).wait_recv()
+            pair(chunk_send.at[0], chunk_recv.at[peer], sem_c, me, peer, device).wait_recv()
+
+    chunks_here()
 
     running = jnp.zeros((16, 128), F32)
     log_sum = jnp.zeros((1, 128), F32)
@@ -306,6 +338,8 @@
     total_send[...] = running.astype(BF16)
     total_log[...] = log_sum
 
+    hear(3)
+
     def far(k, device):
         return (
             pair(total_log, total_log_recv.at[k - 1], sem_tl, k - 1, k - 1, device),
@@ -320,11 +354,15 @@
     for m in range(MEMBERS):
         part_logs[m] = jnp.exp(part_logs[m])
     out_load.wait()
-    for k in range(1, blocks):
-        @pl.when(block >= k)
-        def _():
-            for copy in far(k, sp - k * MEMBERS):
-                copy.wait_recv()
+
+    def totals_here():
+        for k in range(1, blocks):
+            @pl.when(block >= k)
+            def _():
+                for copy in far(k, sp - k * MEMBERS):
+                    copy.wait_recv()
+
+    totals_here()
     incoming = jnp.zeros((16, 128), F32)
     for k in range(blocks - 1, 0, -1):
         incoming = jnp.exp(total_log_recv[k - 1]) * incoming + total_recv[k - 1].astype(F32)
@@ -338,11 +376,15 @@
         copy.start()
         sends.append(copy)
     back_recv[me] = back_send[me]
-    for k in range(1, MEMBERS):
-        peer = (me + k) % MEMBERS
-        pair(
-            back_send.at[0], back_recv.at[peer], sem_b, me, peer, block * MEMBERS + peer
-        ).wait_recv()
+
+    def states_here():
+        for k in range(1, MEMBERS):
+            peer = (me + k) % MEMBERS
+            pair(
+                back_send.at[0], back_recv.at[peer], sem_b, me, peer, block * MEMBERS + peer
+            ).wait_recv()
+
+    states_here()
 
     mixed = []
     for s in range(seqs):
@@ -363,11 +405,15 @@
         copy.start()
         sends.append(copy)
     mix_recv[tp] = mix_send[tp]
-    for k in range(1, 8):
-        peer = (tp + k) % 8
-        remote(
-            mix_send.at[0], mix_recv.at[peer], sem_m.at[0, tp], sem_m.at[1, peer], tp=peer
-        ).wait_recv()
+
+    def heads_here():
+        for k in range(1, 8):
+            peer = (tp + k) % 8
+            remote(
+                mix_send.at[0], mix_recv.at[peer], sem_m.at[0, tp], sem_m.at[1, peer], tp=peer
+            ).wait_recv()
+
+    heads_here()
     rows = jnp.concatenate([mix_recv[t] for t in range(8)], axis=1)
     result = dot(rows, w_out[...])
     out_ref[...] = result.reshape(seqs, 8, result.shape[1]).astype(BF16)
@@ -451,6 +497,7 @@
             dma((2, blocks)),
             dma((2, MEMBERS)),
             dma((2, 8)),
+            pltpu.SemaphoreType.REGULAR((4,)),
         ],
         compiler_params=pltpu.CompilerParams(collective_id=0, has_side_effects=True),
         name="mixer",

time: 64.2 us -> 54 us (0.84)
  Pallas kernels: 62.5 us -> 52.2 us
    pallas_call x1, Pallas kernels: 62.5 us -> 52.2 us  [body(): pl.pallas_call(functools.partial(mixer_kernel, places, seqs), out_shape=j...]
where the time goes in v3:
time: 54 us; the launch traced here: 53.8 us
  Pallas kernels  52.2 us (97%)
  local copies, waits for them, and re-layouts  1.57 us (3%)
    pallas_call x1, Pallas kernels, body(): pl.pallas_call(functools.partial(mixer_kernel, places, seqs), out_shape=j...  52.2 us
    unnamed x1, local copies, waits for them, and re-layouts  1.57 us

profile of v3, /device:TPU:1, one launch (start us, length us, event | category | flops | bytes accessed | tf_op | source)
XLA Modules:
  0.0 53.8 jit_solution(13008251898619436934)
XLA Ops:
  0.0 52.2 %mixer.1 = bf16[4,8,2048]{2,1,0:T(8,128)(2,1)} custom-call(bf16[4,8,2048]{2,1,0:T(8,128)(2,1)} %tokens_ref.1, f32[1,2048]{1,0:T(1,128)} %bitcast.8, bf16[2048,128]{1,0:T(8,128)(2,1)} %gate_ref.1, bf16[2048,128]{1,0:T(8,128)(2,1)} %input_ref.1, bf16[64,2048]{1,0:T(8,128)(2,1)} %bitcast.5, bf16[64,2048]{1,0:T(8,128)(2,1)} %bitcast.6, ...), custom_call_target="tpu_custom_call" | custom-call | tf_op jit(solution)/shard_map/mixer/pallas_call | solution.py:449
  52.2 1.6 %copy.17 = bf16[4,8,2048]{2,1,0:T(8,128)(2,1)} copy(bf16[4,8,2048]{2,1,0:T(8,128)(2,1)} %mixer.1) | data formatting | bytes 262144

commit v4 on v3

v4 whole, which is shorter than its diff:
```python
import functools

import jax
import jax.numpy as jnp
from jax import lax
from jax.experimental import pallas as pl
from jax.experimental.pallas import tpu as pltpu
from jax.sharding import PartitionSpec as P

STATE = 64
NORM_EPS = 1e-06
PRECISE = lax.Precision.HIGHEST
MEMBERS = 16
MESH = pl.DeviceIdType.MESH
F32 = jnp.float32
BF16 = jnp.bfloat16


def rounded(values):
    return values.astype(BF16).astype(F32)


def two_parts(values):
    high = values.astype(BF16)
    return high, (values - high.astype(F32)).astype(BF16)


def three_parts(values):
    high = values.astype(BF16)
    rest = values - high.astype(F32)
    middle = rest.astype(BF16)
    return high, middle, (rest - middle.astype(F32)).astype(BF16)


def silu(values):
    return values / (1.0 + jnp.exp(-values))


def softplus(values):
    return jnp.maximum(values, 0.0) + jnp.log1p(jnp.exp(-jnp.abs(values)))


def dot(a, b, contract=((1,), (0,)), precision=None):
    return lax.dot_general(
        a, b, (contract, ((), ())), precision=precision, preferred_element_type=F32
    )


def mixer_kernel(
    places, seqs,
    tokens_ref, gain_ref, gate_ref, input_ref, key_ref, query_ref, step_ref,
    conv_x_ref, conv_k_ref, conv_q_ref, bias_ref, rate_ref, extra_ref, out_gain_ref,
    out_ref,
    tok, gain, w_gi, w_kq, w_step, conv_x, conv_k, conv_q, bias, rate, extra, out_gain,
    rows_in, tail_out, tail_in,
    gate_s, x_pad, kq_pad, step_s, extra_s,
    xs_s, kq_s, cum_s, inner_s, query_s,
    chunk_send, chunk_recv, log_send, log_recv, part_sums, part_logs,
    total_send, total_log, total_recv, total_log_recv, back_send, back_recv,
    mix_send,
    sem_load, sem_gs, sem_gr, sem_tail, sem_c, sem_l, sem_t, sem_tl, sem_b, sem_m, sem_known,
):
    blocks = places // MEMBERS
    sp, tp = lax.axis_index("sp"), lax.axis_index("tp")
    block, me = sp // MEMBERS, sp % MEMBERS
    chip, core = tp // 2, tp % 2
    ahead, behind = ((chip + 1) % 4) * 2 + core, ((chip + 3) % 4) * 2 + core
    partner = chip * 2 + 1 - core
    place_y = sp % 4
    row_start = sp - place_y

    def along(chips):
        return (sp + 4 * chips + places) % places

    stages = ((1, -1, 2, -2), (4, -4), (8, -8))

    def tell(stage):
        for chips in stages[stage]:
            pl.semaphore_signal(
                sem_known.at[stage], inc=1, device_id={"sp": along(chips)}, device_id_type=MESH
            )

    def hear(stage):
        pl.semaphore_wait(sem_known.at[stage], len(stages[stage]))
        pl.semaphore_signal(
            sem_known.at[stage], inc=1, device_id={"tp": partner}, device_id_type=MESH
        )
        if stage + 1 < len(stages):
            tell(stage + 1)

    def relay(stage):
        @pl.when(core == 1)
        def _():
            hear(stage)

    def learn(stage):
        @pl.when(core == 0)
        def _():
            pl.semaphore_wait(sem_known.at[stage], 1)

    def load(k, source, target):
        copy = pltpu.make_async_copy(source, target, sem_load.at[k])
        copy.start()
        return copy

    tok_load = load(0, tokens_ref, tok)

    def remote(source, target, send_sem, recv_sem, **device):
        return pltpu.make_async_remote_copy(
            src_ref=source, dst_ref=target, send_sem=send_sem, recv_sem=recv_sem,
            device_id=device, device_id_type=MESH,
        )

    def pair(source, target, sems, device):
        return remote(source, target, sems.at[0], sems.at[1], sp=device)

    def all_done(buffer, sem):
        pltpu.make_async_copy(buffer, buffer, sem).wait()

    for k in range(blocks - 1):
        total_recv[k] = jnp.zeros((16, 128), BF16)
        total_log_recv[k] = jnp.zeros((1, 128), F32)

    @pl.when(sp == 0)
    def _():
        tail_in[...] = jnp.zeros_like(tail_in)

    barrier = pltpu.get_barrier_semaphore()

    def greet(**device):
        pl.semaphore_signal(barrier, inc=1, device_id=device, device_id_type=MESH)

    for k in range(1, 8):
        greet(tp=(tp + k) % 8)
    for k in range(1, 4):
        greet(sp=row_start + (place_y + k) % 4, tp=chip * 2 + 1)
    for chips in stages[0]:
        greet(sp=along(chips), tp=chip * 2 + 1)

    from_tail = (core == 1) & (chip != 1)

    @pl.when((sp > 0) & from_tail)
    def _():
        greet(sp=sp - 1, tp=7)

    weight_loads = [
        load(1, gain_ref, gain),
        load(2, step_ref, w_step),
        load(3, extra_ref, extra),
        load(4, gate_ref, w_gi.at[:, 0:128]),
        load(4, input_ref, w_gi.at[:, 128:256]),
        load(5, key_ref, w_kq.at[0:64, :]),
        load(5, query_ref, w_kq.at[64:128, :]),
        load(6, conv_x_ref, conv_x),
        load(7, conv_k_ref, conv_k),
        load(8, conv_q_ref, conv_q),
        load(9, bias_ref, bias),
        load(10, rate_ref, rate),
        load(11, out_gain_ref, out_gain),
    ]
    gain_load, step_load, extra_load = weight_loads[0:3]
    weight_loads = weight_loads[7:]

    tok_load.wait()
    gain_load.wait()
    values = tok[...].astype(F32)
    mean_sq = jnp.mean(values * values, axis=-1, keepdims=True)
    normed = values * lax.rsqrt(mean_sq + NORM_EPS) * gain[...]
    rows_in[0] = normed.reshape(seqs * 8, tok.shape[2]).astype(BF16)

    has_tail = (tp == 7) & (sp + 1 < places)

    @pl.when(has_tail)
    def _():
        tail_out[...] = normed[:, 4:8, :].reshape(seqs * 4, tok.shape[2]).astype(BF16)

    def entry():
        @pl.when(core == 0)
        def _():
            pl.semaphore_wait(barrier, 7)

        @pl.when((core == 1) & ~has_tail)
        def _():
            pl.semaphore_wait(barrier, 7 + 6 + 8)

        @pl.when(has_tail)
        def _():
            pl.semaphore_wait(barrier, 7 + 6 + 8 + 3)

    entry()

    width = tok.shape[2]

    def quarter(slot, part):
        columns = pl.ds(part % 2 * (width // 2), width // 2)
        return rows_in.at[slot, pl.ds(part // 2 * 16, 16), columns]

    def landing(slot, part):
        if slot in (4, 5, 6):
            return sem_gr.at[(slot - 4) * 4 + part]
        return sem_gr.at[12 if slot < 4 else 13]

    def pass_on(slot, part, to_slot, device):
        remote(
            quarter(slot, part), quarter(to_slot, part),
            sem_gs.at[0], landing(to_slot, part), tp=device,
        ).start()

    def arrived(slot, *parts):
        for part in parts:
            all_done(quarter(slot, part), landing(slot, part))

    for part in range(4):
        pass_on(0, part, 5, ahead)
        pass_on(0, (part + 2) % 4, 4, behind)
    for part in range(4):
        pass_on(0, part, 1, partner)

    def tail(k, source, **device):
        return remote(source, tail_in, sem_tail.at[k], sem_tail.at[5], **device)

    @pl.when(has_tail)
    def _():
        for k, target in enumerate((7, 1, 5)):
            tail(k, tail_out, sp=sp + 1, tp=target).start()

    @pl.when(core == 1)
    def _():
        tell(0)

    row = lax.broadcasted_iota(jnp.int32, (64, 128), 0)
    lane = lax.broadcasted_iota(jnp.int32, (64, 128), 1)
    inside = lane % 64
    diagonal = row == inside
    causal = row >= inside
    first_head = lane < 64
    lane_row = lax.broadcasted_iota(jnp.int32, (1, 128), 1)

    step_load.wait()
    extra_load.wait()
    pick_row = lax.broadcasted_iota(jnp.int32, (128, 16), 0) // 64 + 2 * tp
    pick = (pick_row == lax.broadcasted_iota(jnp.int32, (128, 16), 1)).astype(F32).astype(BF16)
    w_kq[128:256, :] = dot(pick, w_step[...]).astype(BF16)
    same_head = (
        lax.broadcasted_iota(jnp.int32, (128, 128), 0) // 64
        == lax.broadcasted_iota(jnp.int32, (128, 128), 1) // 64
    ).astype(F32)
    for s in range(seqs):
        extra_row = jnp.concatenate([extra[s, 0:1, :], extra[s, 1:2, :]], axis=1)
        extra_s[s] = dot(jnp.where(diagonal, extra_row, 0.0), same_head, precision=PRECISE)
    all_done(w_gi, sem_load.at[4])
    all_done(w_kq.at[pl.ds(0, 128)], sem_load.at[5])
    for copy in weight_loads:
        copy.wait()
    bias_row = jnp.where(lane_row < 64, bias[:, 0:1], bias[:, 1:2])
    rate_row = jnp.where(lane_row < 64, rate[:, 0:1], rate[:, 1:2])
    relay(0)

    arrived(5, 0)
    pass_on(5, 0, 6, ahead)
    arrived(4, 2)
    pass_on(4, 2, 6, behind)
    arrived(5, 1)
    pass_on(5, 1, 6, ahead)
    arrived(4, 3)
    pass_on(4, 3, 6, behind)
    for part in (0, 1):
        pass_on(5, part, 3, partner)
        pass_on(4, part + 2, 2, partner)

    def tail_first():
        @pl.when((sp > 0) & from_tail)
        def _():
            tail(0, tail_out, tp=partner).wait_recv()
            tail(4, tail_in, tp=partner).start()

            @pl.when(chip == 0)
            def _():
                tail(3, tail_in, tp=ahead).start()

    for part in (2, 3):
        arrived(5, part)
        pass_on(5, part, 3, partner)
    for part in (0, 1):
        arrived(4, part)
        pass_on(4, part, 2, partner)
    tail_first()
    def opposite_rows():
        for part in range(4):
            arrived(6, part)
            pass_on(6, part, 7, partner)

    def partner_rows():
        all_done(rows_in.at[pl.ds(1, 3)], sem_gr.at[12])

    position = [
        ((chip + away) % 4) * 2 + (core if same else 1 - core)
        for away, same in (
            (0, True), (0, False), (1, False), (3, False),
            (1, True), (3, True), (2, True), (2, False),
        )
    ]

    def project(first, count, more=()):
        rows = rows_in[first : first + count].reshape(count * 32, width)
        rows = jnp.concatenate([rows, *more], axis=0)
        gate_x = rounded(dot(rows, w_gi[...]))
        kq_step = rounded(dot(rows, w_kq[...], ((1,), (1,))))
        for i in range(count):
            at = pl.multiple_of(position[first + i] * 8, 8)
            for s in range(seqs):
                part = slice(i * 32 + s * 8, i * 32 + s * 8 + 8)
                gate_s[s, pl.ds(at, 8), :] = gate_x[part, 0:128]
                x_pad[s, pl.ds(at + 8, 8), :] = gate_x[part, 128:256]
                kq_pad[s, pl.ds(at + 8, 8), :] = kq_step[part, 0:128]
                step_s[s, pl.ds(at, 8), :] = kq_step[part, 128:256]
        if more:
            for s in range(seqs):
                part = slice(count * 32 + s * 4 + 1, count * 32 + s * 4 + 4)
                x_pad[s, 5:8, :] = gate_x[part, 128:256]
                kq_pad[s, 5:8, :] = kq_step[part, 0:128]

    def tail_last():
        @pl.when((sp > 0) & (core == 1) & (chip == 1))
        def _():
            tail(0, tail_out, tp=partner).wait_recv()
            tail(4, tail_in, tp=partner).start()

        @pl.when((sp > 0) & (core == 0))
        def _():
            tail(0, tail_out, tp=partner).wait_recv()

    relay(1)

    @pl.when(core == 1)
    def _():
        opposite_rows()

    partner_rows()
    project(0, 6)

    @pl.when(core == 0)
    def _():
        opposite_rows()

    def last_rows():
        all_done(rows_in.at[7], sem_gr.at[13])

    last_rows()
    tail_last()
    project(6, 2, (tail_in[...],))
    triangle = (
        lax.broadcasted_iota(jnp.int32, (64, 192), 0)
        >= lax.broadcasted_iota(jnp.int32, (64, 192), 1) % 64
    ).astype(F32).astype(BF16)
    for s in range(seqs):
        step = softplus(step_s[s] + bias_row)
        step_s[s] = step
        log_decay = extra_s[s] - step * rate_row
        cum = dot(triangle, jnp.concatenate(three_parts(log_decay), axis=0))
        cum_s[s] = cum
        log_send[s] = cum[63:64, :]

    def members():
        for k in range(1, MEMBERS):
            peer = (me + k) % MEMBERS
            yield peer, block * MEMBERS + peer

    learn(0)
    learn(1)
    for peer, device in members():
        copy = pair(log_send.at[peer // 4], log_recv.at[me], sem_l, device)
        copy.start()
    log_recv[me] = log_send[me // 4]

    conv_kq = jnp.concatenate([conv_k[...], conv_q[...]], axis=1)
    for s in range(seqs):
        x_sum = x_pad[s, 5:69, :] * conv_x[0:1, :]
        kq_sum = kq_pad[s, 5:69, :] * conv_kq[0:1, :]
        for k in range(1, 4):
            x_sum = x_sum + x_pad[s, 5 + k : 69 + k, :] * conv_x[k : k + 1, :]
            kq_sum = kq_sum + kq_pad[s, 5 + k : 69 + k, :] * conv_kq[k : k + 1, :]
        scaled = silu(x_sum) * step_s[s]
        kq = silu(kq_sum)
        xs_s[s] = scaled
        kq_s[s] = kq
        cum = cum_s[s]
        x_high, x_low = two_parts(scaled * jnp.exp(cum[63:64, :] - cum))
        k_high, k_low = two_parts(kq[:, 0:64])
        state = dot(
            jnp.concatenate([k_high, k_high, k_low], axis=0),
            jnp.concatenate([x_high, x_low, x_high], axis=0),
            ((0,), (0,)),
        )
        for q in range(4):
            chunk_send[s * 4 + q] = state[q * 16 : q * 16 + 16, :].astype(BF16)

    for peer, device in members():
        copy = pair(chunk_send.at[peer], chunk_recv.at[me], sem_c, device)
        copy.start()
    chunk_recv[me] = chunk_send[me]

    for s in range(seqs):
        cum, kq, scaled = cum_s[s], kq_s[s], xs_s[s]
        keys, queries = kq[:, 0:64], kq[:, 64:128]
        query_s[s] = jnp.concatenate(two_parts(queries), axis=1)
        cum_row = jnp.sum(jnp.where(diagonal, cum, 0.0), axis=0, keepdims=True)
        decay = jnp.where(causal, jnp.exp(jnp.where(causal, cum - cum_row, 0.0)), 0.0)
        scores = dot(queries, jnp.concatenate([keys, keys], axis=0), ((1,), (1,)), PRECISE)
        apart = jnp.concatenate(
            [jnp.where(first_head, scaled, 0.0), jnp.where(first_head, 0.0, scaled)], axis=0
        )
        inner_s[s] = dot(scores * decay, apart, precision=PRECISE)
        cum_s[s] = jnp.exp(cum)
        gate_s[s] = silu(gate_s[s])

    def logs_here():
        all_done(log_recv.at[pl.ds(0, MEMBERS - 1)], sem_l.at[1])

    def chunks_here():
        all_done(chunk_recv.at[pl.ds(0, MEMBERS - 1)], sem_c.at[1])

    def far_log(k, device):
        return pair(total_log, total_log_recv.at[k - 1], sem_tl, device)

    def far(k, device):
        return pair(total_send, total_recv.at[k - 1], sem_t, device)

    def later_blocks(act):
        for k in range(1, blocks):
            @pl.when(block + k < blocks)
            def _():
                act(k, sp + k * MEMBERS)

    def count_done(count, side):
        for k in range(1, blocks):
            @pl.when(count == k)
            def _():
                all_done(total_log_recv.at[pl.ds(0, k)], sem_tl.at[side])
                all_done(total_recv.at[pl.ds(0, k)], sem_t.at[side])

    def rows_sent():
        all_done(rows_in.at[pl.ds(0, 7)], sem_gs.at[0])

        @pl.when(has_tail)
        def _():
            for k in range(3):
                tail(k, tail_out, sp=sp + 1, tp=7).wait_send()

        @pl.when((sp > 0) & (core == 1))
        def _():
            tail(4, tail_in, tp=partner).wait_send()

            @pl.when(chip == 0)
            def _():
                tail(3, tail_in, tp=ahead).wait_send()

    rows_sent()

    logs_here()
    log_sum = jnp.zeros((1, 128), F32)
    for m in range(MEMBERS):
        part_logs[m] = jnp.exp(log_sum)
        log_sum = log_sum + log_recv[m]
        log_recv[m] = jnp.exp(log_recv[m])
    total_log[...] = log_sum
    chunks_here()
    running = jnp.zeros((16, 128), F32)
    for m in range(MEMBERS):
        part_sums[m] = running
        running = log_recv[m] * running + chunk_recv[m].astype(F32)
    total_send[...] = running.astype(BF16)
    relay(2)
    learn(2)
    later_blocks(lambda k, device: far_log(k, device).start())
    later_blocks(lambda k, device: far(k, device).start())

    def totals_here():
        count_done(block, 1)

    totals_here()
    incoming = jnp.zeros((16, 128), F32)
    for k in range(blocks - 1, 0, -1):
        incoming = jnp.exp(total_log_recv[k - 1]) * incoming + total_recv[k - 1].astype(F32)
    for m in range(MEMBERS):
        back_send[m] = (part_sums[m] + part_logs[m] * incoming).astype(BF16)
    for peer, device in members():
        copy = pair(back_send.at[peer], back_recv.at[me], sem_b, device)
        copy.start()
    back_recv[me] = back_send[me]

    def parts_sent():
        all_done(log_recv.at[pl.ds(0, MEMBERS - 1)], sem_l.at[0])
        all_done(chunk_recv.at[pl.ds(0, MEMBERS - 1)], sem_c.at[0])
        all_done(back_recv.at[pl.ds(0, MEMBERS - 1)], sem_b.at[0])
        count_done(blocks - 1 - block, 0)

    parts_sent()

    def states_here():
        all_done(back_recv.at[pl.ds(0, MEMBERS - 1)], sem_b.at[1])

    states_here()

    mixed = []
    for s in range(seqs):
        state = back_recv[s * 4 : s * 4 + 4].reshape(64, 128)
        carried = dot(query_s[s], jnp.concatenate([state, state], axis=0))
        gated = (inner_s[s] + carried * cum_s[s]) * gate_s[s]
        mean_sq = jnp.mean(gated * gated, axis=-1, keepdims=True)
        mixed.append(gated * lax.rsqrt(mean_sq + NORM_EPS) * out_gain[...])
    for t in range(8):
        mix_send[t] = jnp.concatenate(
            [part[t * 8 : t * 8 + 8, :] for part in mixed], axis=0
        ).astype(BF16)

    def columns(source):
        return out_ref.at[:, pl.ds(pl.multiple_of(source * 128, 128), 128)]

    for k in range(1, 8):
        peer = (tp + k) % 8
        copy = remote(
            mix_send.at[peer], columns(tp), sem_m.at[0], sem_m.at[1], tp=peer
        )
        copy.start()
    own = pltpu.make_async_copy(mix_send.at[tp], columns(tp), sem_m.at[2])
    own.start()

    def heads_here():
        all_done(mix_send.at[pl.ds(0, 7)], sem_m.at[1])

    heads_here()
    def heads_sent():
        own.wait()
        all_done(mix_send.at[pl.ds(0, 7)], sem_m.at[0])

    heads_sent()


def body(
    tokens, in_gain, gate_weight, input_weight, key_weight, query_weight, step_weight,
    conv_input, conv_key, conv_query, step_bias, decay_rate, decay_extra, out_gain, out_weight,
):
    places = lax.axis_size("sp")
    blocks = places // MEMBERS
    seqs, _, width = tokens.shape
    inner = out_weight.shape[0]
    local = (seqs, 64, 128)
    padded = (seqs, 72, 128)
    dma = pltpu.SemaphoreType.DMA
    vmem = pltpu.VMEM
    operands = (
        tokens, in_gain.reshape(1, width), gate_weight, input_weight, key_weight.T,
        query_weight.T, step_weight.T, conv_input, conv_key, conv_query,
        step_bias.reshape(1, 2), decay_rate.reshape(1, 2), decay_extra,
        out_gain.reshape(1, 128),
    )
    rows = pl.pallas_call(
        functools.partial(mixer_kernel, places, seqs),
        out_shape=jax.ShapeDtypeStruct((seqs * 8, inner), BF16),
        in_specs=[pl.BlockSpec(memory_space=pl.ANY)] * 14,
        out_specs=pl.BlockSpec(memory_space=pl.ANY),
        scratch_shapes=[
            vmem(tokens.shape, BF16),
            vmem((1, width), F32),
            vmem((width, 256), BF16),
            vmem((256, width), BF16),
            vmem((16, width), BF16),
            vmem(conv_input.shape, F32),
            vmem(conv_key.shape, F32),
            vmem(conv_query.shape, F32),
            vmem((1, 2), F32),
            vmem((1, 2), F32),
            vmem(decay_extra.shape, F32),
            vmem((1, 128), F32),
            vmem((8, seqs * 8, width), BF16),
            vmem((seqs * 4, width), BF16),
            vmem((seqs * 4, width), BF16),
            vmem(local, F32),
            vmem(padded, F32),
            vmem(padded, F32),
            vmem(local, F32),
            vmem(local, F32),
            vmem(local, F32),
            vmem(local, F32),
            vmem(local, F32),
            vmem(local, F32),
            vmem(local, BF16),
            vmem((MEMBERS, 16, 128), BF16),
            vmem((MEMBERS, 16, 128), BF16),
            vmem((seqs, 1, 128), F32),
            vmem((MEMBERS, 1, 128), F32),
            vmem((MEMBERS, 16, 128), F32),
            vmem((MEMBERS, 1, 128), F32),
            vmem((16, 128), BF16),
            vmem((1, 128), F32),
            vmem((blocks - 1, 16, 128), BF16),
            vmem((blocks - 1, 1, 128), F32),
            vmem((MEMBERS, 16, 128), BF16),
            vmem((MEMBERS, 16, 128), BF16),
            vmem((8, seqs * 8, 128), BF16),
            dma((12,)),
            dma((1,)),
            dma((14,)),
            dma((6,)),
            dma((2,)),
            dma((2,)),
            dma((2,)),
            dma((2,)),
            dma((2,)),
            dma((3,)),
            pltpu.SemaphoreType.REGULAR((3,)),
        ],
        compiler_params=pltpu.CompilerParams(
            collective_id=0, has_side_effects=True, vmem_limit_bytes=16 * 2**20
        ),
        cost_estimate=pl.CostEstimate(
            flops=4 * 10**9, bytes_accessed=2 * 2**20, transcendentals=0
        ),
        name="mixer",
    )(*[pltpu.with_memory_space_constraint(operand, pltpu.HBM) for operand in operands])
    result = jnp.dot(rows, out_weight, preferred_element_type=F32)
    return result.astype(BF16).reshape(tokens.shape)


def solution(mesh):
    placed = (
        P(None, ("sp", "tp"), None),
        P(),
        P(None, "tp"),
        P(None, "tp"),
        P(None, "tp"),
        P(None, "tp"),
        P(),
        P(None, "tp"),
        P(None, "tp"),
        P(None, "tp"),
        P("tp"),
        P("tp"),
        P(None, "tp", "sp"),
        P("tp"),
        P(),
    )
    return jax.shard_map(
        body, mesh=mesh, in_specs=placed, out_specs=P(None, ("sp", "tp"), None), check_vma=False
    )
```

time: 54 us -> 46.6 us (0.86)
  Pallas kernels: 52.2 us -> 45 us
  local copies, waits for them, and re-layouts: 1.57 us -> 0.01 us
  matrix products: 0 us -> 1.49 us
    pallas_call x1, Pallas kernels: 52.2 us -> 45 us  [body(): pl.pallas_call(functools.partial(mixer_kernel, places, seqs), out_shape=j...]
    unnamed x1 -> x2, local copies, waits for them, and re-layouts: 1.57 us -> 0.01 us
    dot_general x0 -> x1, matrix products: none -> 1.49 us  [body(): result = jnp.dot(rows, out_weight, preferred_element_type=F32)]
where the time goes in v4:
time: 46.6 us; the launch traced here: 46.5 us
  Pallas kernels  45 us (97%)
  matrix products  1.49 us (3%)
    pallas_call x1, Pallas kernels, body(): pl.pallas_call(functools.partial(mixer_kernel, places, seqs), out_shape=j...  45 us
    dot_general x1, matrix products, body(): result = jnp.dot(rows, out_weight, preferred_element_type=F32)  1.49 us

profile of v4, /device:TPU:1, one launch (start us, length us, event | category | flops | bytes accessed | tf_op | source)
XLA Modules:
  0.0 46.5 jit_solution(17120145289165351012)
XLA Ops:
  0.0 0.0 copy-start
  0.0 45.0 %mixer.1 = bf16[32,1024]{1,0:T(8,128)(2,1)S(1)} custom-call(bf16[4,8,2048]{2,1,0:T(8,128)(2,1)} %tokens_ref.1, f32[1,2048]{1,0:T(1,128)} %bitcast.14, bf16[2048,128]{1,0:T(8,128)(2,1)} %gate_ref.1, bf16[2048,128]{1,0:T(8,128)(2,1)} %input_ref.1, bf16[64,2048]{1,0:T(8,128)(2,1)} %bitcast.11, bf16[64,2048]{1,0:T(8,128)(2,1)} %bitcast.12, ...), custom_call_target="tpu_custom_call" | custom-call | flops 4000000000 | bytes 2097152 | tf_op jit(solution)/shard_map/mixer/pallas_call | solution.py:558
  45.0 0.0 copy-done
  45.0 1.5 %fusion = bf16[4,8,2048]{2,1,0:T(8,128)(2,1)} fusion(bf16[32,1024]{1,0:T(8,128)(2,1)S(1)} %mixer.1, bf16[1024,2048]{1,0:T(8,128)(2,1)S(1)} %copy-done), kind=kOutput, calls=%fused_computation.1 | convolution fusion | flops 134283264 | bytes 4390912 | tf_op jit(solution)/shard_map/dot_general | solution.py:622
Async XLA Ops:
  0.0 45.0 %copy-start = (bf16[1024,2048]{1,0:T(8,128)(2,1)S(1)}, bf16[1024,2048]{1,0:T(8,128)(2,1)}, u32[]{:S(2)}) copy-start(bf16[1024,2048]{1,0:T(8,128)(2,1)} %param.29) | copy-start | bytes 12582916

commit v5 on v4

--- a/solution.py
+++ b/solution.py
@@ -178,7 +178,15 @@
         @pl.when(core == 0)
         def _():
             pl.semaphore_wait(barrier, 7)
-
+            pl.semaphore_signal(
+                sem_known.at[3], inc=1, device_id={"tp": partner}, device_id_type=MESH
+            )
+
+        @pl.when(core == 1)
+        def _():
+            pl.semaphore_wait(sem_known.at[3], 1)
+
+    def entry_near():
         @pl.when((core == 1) & ~has_tail)
         def _():
             pl.semaphore_wait(barrier, 7 + 6 + 8)
@@ -218,15 +226,6 @@
 
     def tail(k, source, **device):
         return remote(source, tail_in, sem_tail.at[k], sem_tail.at[5], **device)
-
-    @pl.when(has_tail)
-    def _():
-        for k, target in enumerate((7, 1, 5)):
-            tail(k, tail_out, sp=sp + 1, tp=target).start()
-
-    @pl.when(core == 1)
-    def _():
-        tell(0)
 
     row = lax.broadcasted_iota(jnp.int32, (64, 128), 0)
     lane = lax.broadcasted_iota(jnp.int32, (64, 128), 1)
@@ -248,14 +247,23 @@
     for s in range(seqs):
         extra_row = jnp.concatenate([extra[s, 0:1, :], extra[s, 1:2, :]], axis=1)
         extra_s[s] = dot(jnp.where(diagonal, extra_row, 0.0), same_head, precision=PRECISE)
+    entry_near()
+
+    @pl.when(has_tail)
+    def _():
+        for k, target in enumerate((7, 1, 5)):
+            tail(k, tail_out, sp=sp + 1, tp=target).start()
+
+    @pl.when(core == 1)
+    def _():
+        tell(0)
+
     all_done(w_gi, sem_load.at[4])
     all_done(w_kq.at[pl.ds(0, 128)], sem_load.at[5])
     for copy in weight_loads:
         copy.wait()
     bias_row = jnp.where(lane_row < 64, bias[:, 0:1], bias[:, 1:2])
     rate_row = jnp.where(lane_row < 64, rate[:, 0:1], rate[:, 1:2])
-    relay(0)
-
     arrived(5, 0)
     pass_on(5, 0, 6, ahead)
     arrived(4, 2)
@@ -267,7 +275,6 @@
     for part in (0, 1):
         pass_on(5, part, 3, partner)
         pass_on(4, part + 2, 2, partner)
-
     def tail_first():
         @pl.when((sp > 0) & from_tail)
         def _():
@@ -284,6 +291,7 @@
     for part in (0, 1):
         arrived(4, part)
         pass_on(4, part, 2, partner)
+    relay(0)
     tail_first()
     def opposite_rows():
         for part in range(4):
@@ -330,11 +338,10 @@
         def _():
             tail(0, tail_out, tp=partner).wait_recv()
 
-    relay(1)
-
     @pl.when(core == 1)
     def _():
         opposite_rows()
+
 
     partner_rows()
     project(0, 6)
@@ -362,10 +369,13 @@
         log_send[s] = cum[63:64, :]
 
     def members():
-        for k in range(1, MEMBERS):
-            peer = (me + k) % MEMBERS
-            yield peer, block * MEMBERS + peer
-
+        for chips in (3, 1, 2, 0):
+            for k in (2, 1, 3, 0):
+                if chips or k:
+                    peer = (me // 4 + chips) % 4 * 4 + (me + k) % 4
+                    yield peer, block * MEMBERS + peer
+
+    relay(1)
     learn(0)
     learn(1)
     for peer, device in members():
@@ -427,7 +437,7 @@
         return pair(total_send, total_recv.at[k - 1], sem_t, device)
 
     def later_blocks(act):
-        for k in range(1, blocks):
+        for k in sorted(range(1, blocks), key=lambda k: abs(2 * k - blocks)):
             @pl.when(block + k < blocks)
             def _():
                 act(k, sp + k * MEMBERS)
@@ -472,8 +482,12 @@
     total_send[...] = running.astype(BF16)
     relay(2)
     learn(2)
-    later_blocks(lambda k, device: far_log(k, device).start())
-    later_blocks(lambda k, device: far(k, device).start())
+
+    def send_far(k, device):
+        far_log(k, device).start()
+        far(k, device).start()
+
+    later_blocks(send_far)
 
     def totals_here():
         count_done(block, 1)
@@ -517,12 +531,13 @@
     def columns(source):
         return out_ref.at[:, pl.ds(pl.multiple_of(source * 128, 128), 128)]
 
-    for k in range(1, 8):
-        peer = (tp + k) % 8
-        copy = remote(
-            mix_send.at[peer], columns(tp), sem_m.at[0], sem_m.at[1], tp=peer
-        )
-        copy.start()
+    for chips in (2, 1, 3, 0):
+        for same in (True, False):
+            if chips or not same:
+                peer = (chip + chips) % 4 * 2 + (core if same else 1 - core)
+                remote(
+                    mix_send.at[peer], columns(tp), sem_m.at[0], sem_m.at[1], tp=peer
+                ).start()
     own = pltpu.make_async_copy(mix_send.at[tp], columns(tp), sem_m.at[2])
     own.start()
 
@@ -609,7 +624,7 @@
             dma((2,)),
             dma((2,)),
             dma((3,)),
-            pltpu.SemaphoreType.REGULAR((3,)),
+            pltpu.SemaphoreType.REGULAR((4,)),
         ],
         compiler_params=pltpu.CompilerParams(
             collective_id=0, has_side_effects=True, vmem_limit_bytes=16 * 2**20

time: 46.6 us -> 49.3 us (1.058)
  Pallas kernels: 45 us -> 47.7 us
    pallas_call x1, Pallas kernels: 45 us -> 47.7 us  [body(): pl.pallas_call(functools.partial(mixer_kernel, places, seqs), out_shape=j...]
where the time goes in v5:
time: 49.3 us; the launch traced here: 49.2 us
  Pallas kernels  47.7 us (97%)
  matrix products  1.49 us (3%)
    pallas_call x1, Pallas kernels, body(): pl.pallas_call(functools.partial(mixer_kernel, places, seqs), out_shape=j...  47.7 us
    dot_general x1, matrix products, body(): result = jnp.dot(rows, out_weight, preferred_element_type=F32)  1.49 us

profile of v5, /device:TPU:1, one launch (start us, length us, event | category | flops | bytes accessed | tf_op | source)
XLA Modules:
  0.0 49.2 jit_solution(8931434369798645607)
XLA Ops:
  0.0 0.0 copy-start
  0.0 47.7 %mixer.1 = bf16[32,1024]{1,0:T(8,128)(2,1)S(1)} custom-call(bf16[4,8,2048]{2,1,0:T(8,128)(2,1)} %tokens_ref.1, f32[1,2048]{1,0:T(1,128)} %bitcast.14, bf16[2048,128]{1,0:T(8,128)(2,1)} %gate_ref.1, bf16[2048,128]{1,0:T(8,128)(2,1)} %input_ref.1, bf16[64,2048]{1,0:T(8,128)(2,1)} %bitcast.11, bf16[64,2048]{1,0:T(8,128)(2,1)} %bitcast.12, ...), custom_call_target="tpu_custom_call" | custom-call | flops 4000000000 | bytes 2097152 | tf_op jit(solution)/shard_map/mixer/pallas_call | solution.py:573
  47.7 0.0 copy-done
  47.7 1.5 %fusion = bf16[4,8,2048]{2,1,0:T(8,128)(2,1)} fusion(bf16[32,1024]{1,0:T(8,128)(2,1)S(1)} %mixer.1, bf16[1024,2048]{1,0:T(8,128)(2,1)S(1)} %copy-done), kind=kOutput, calls=%fused_computation.1 | convolution fusion | flops 134283264 | bytes 4390912 | tf_op jit(solution)/shard_map/dot_general | solution.py:637
Async XLA Ops:
  0.0 47.7 %copy-start = (bf16[1024,2048]{1,0:T(8,128)(2,1)S(1)}, bf16[1024,2048]{1,0:T(8,128)(2,1)}, u32[]{:S(2)}) copy-start(bf16[1024,2048]{1,0:T(8,128)(2,1)} %param.29) | copy-start | bytes 12582916

commit v6 on v5

--- a/solution.py
+++ b/solution.py
@@ -227,6 +227,17 @@
     def tail(k, source, **device):
         return remote(source, tail_in, sem_tail.at[k], sem_tail.at[5], **device)
 
+    entry_near()
+
+    @pl.when(has_tail)
+    def _():
+        for k, target in enumerate((7, 1, 5)):
+            tail(k, tail_out, sp=sp + 1, tp=target).start()
+
+    @pl.when(core == 1)
+    def _():
+        tell(0)
+
     row = lax.broadcasted_iota(jnp.int32, (64, 128), 0)
     lane = lax.broadcasted_iota(jnp.int32, (64, 128), 1)
     inside = lane % 64
@@ -247,23 +258,14 @@
     for s in range(seqs):
         extra_row = jnp.concatenate([extra[s, 0:1, :], extra[s, 1:2, :]], axis=1)
         extra_s[s] = dot(jnp.where(diagonal, extra_row, 0.0), same_head, precision=PRECISE)
-    entry_near()
-
-    @pl.when(has_tail)
-    def _():
-        for k, target in enumerate((7, 1, 5)):
-            tail(k, tail_out, sp=sp + 1, tp=target).start()
-
-    @pl.when(core == 1)
-    def _():
-        tell(0)
-
     all_done(w_gi, sem_load.at[4])
     all_done(w_kq.at[pl.ds(0, 128)], sem_load.at[5])
     for copy in weight_loads:
         copy.wait()
     bias_row = jnp.where(lane_row < 64, bias[:, 0:1], bias[:, 1:2])
     rate_row = jnp.where(lane_row < 64, rate[:, 0:1], rate[:, 1:2])
+    relay(0)
+
     arrived(5, 0)
     pass_on(5, 0, 6, ahead)
     arrived(4, 2)
@@ -291,7 +293,6 @@
     for part in (0, 1):
         arrived(4, part)
         pass_on(4, part, 2, partner)
-    relay(0)
     tail_first()
     def opposite_rows():
         for part in range(4):
@@ -338,6 +339,8 @@
         def _():
             tail(0, tail_out, tp=partner).wait_recv()
 
+    relay(1)
+
     @pl.when(core == 1)
     def _():
         opposite_rows()
@@ -375,7 +378,6 @@
                     peer = (me // 4 + chips) % 4 * 4 + (me + k) % 4
                     yield peer, block * MEMBERS + peer
 
-    relay(1)
     learn(0)
     learn(1)
     for peer, device in members():

time: 49.3 us -> 46.6 us (0.945)
  Pallas kernels: 47.7 us -> 45 us
    pallas_call x1, Pallas kernels: 47.7 us -> 45 us  [body(): pl.pallas_call(functools.partial(mixer_kernel, places, seqs), out_shape=j...]
where the time goes in v6:
time: 46.6 us; the launch traced here: 46.5 us
  Pallas kernels  45 us (97%)
  matrix products  1.49 us (3%)
    pallas_call x1, Pallas kernels, body(): pl.pallas_call(functools.partial(mixer_kernel, places, seqs), out_shape=j...  45 us
    dot_general x1, matrix products, body(): result = jnp.dot(rows, out_weight, preferred_element_type=F32)  1.49 us

profile of v6, /device:TPU:1, one launch (start us, length us, event | category | flops | bytes accessed | tf_op | source)
XLA Modules:
  0.0 46.5 jit_solution(2041276808343605574)
XLA Ops:
  0.0 0.0 copy-start
  0.0 45.0 %mixer.1 = bf16[32,1024]{1,0:T(8,128)(2,1)S(1)} custom-call(bf16[4,8,2048]{2,1,0:T(8,128)(2,1)} %tokens_ref.1, f32[1,2048]{1,0:T(1,128)} %bitcast.14, bf16[2048,128]{1,0:T(8,128)(2,1)} %gate_ref.1, bf16[2048,128]{1,0:T(8,128)(2,1)} %input_ref.1, bf16[64,2048]{1,0:T(8,128)(2,1)} %bitcast.11, bf16[64,2048]{1,0:T(8,128)(2,1)} %bitcast.12, ...), custom_call_target="tpu_custom_call" | custom-call | flops 4000000000 | bytes 2097152 | tf_op jit(solution)/shard_map/mixer/pallas_call | solution.py:575
  45.0 0.0 copy-done
  45.0 1.5 %fusion = bf16[4,8,2048]{2,1,0:T(8,128)(2,1)} fusion(bf16[32,1024]{1,0:T(8,128)(2,1)S(1)} %mixer.1, bf16[1024,2048]{1,0:T(8,128)(2,1)S(1)} %copy-done), kind=kOutput, calls=%fused_computation.1 | convolution fusion | flops 134283264 | bytes 4390912 | tf_op jit(solution)/shard_map/dot_general | solution.py:639
Async XLA Ops:
  0.0 45.0 %copy-start = (bf16[1024,2048]{1,0:T(8,128)(2,1)S(1)}, bf16[1024,2048]{1,0:T(8,128)(2,1)}, u32[]{:S(2)}) copy-start(bf16[1024,2048]{1,0:T(8,128)(2,1)} %param.29) | copy-start | bytes 12582916
